TPU v7x, 128 devices: a whole 4x4x4 slice. The times are simulated.
128 devices in a mesh: ep: 32 (over z, y, core), tp: 4 (over x).
Axes of the slice: x: 4, y: 4, z: 4, core: 2. Of those that a mesh axis runs over, the one named last changes fastest.
Arguments:
- query_rows: bfloat16 [16384, 1024], P('ep', 'tp'), may hold values from -10 to 10
- key_rows: bfloat16 [16384, 1024], P('ep', 'tp'), may hold values from -10 to 10
- value_rows: bfloat16 [16384, 1024], P('ep', 'tp'), may hold values from -6 to 6
- key_bias: float32 [16384, 16], P(None, 'tp'), may hold values from -30 to 0
- out_weight: bfloat16 [1024, 2048], P('tp'), may hold values from -0.5625 to 0.5625
- moe_input: bfloat16 [16384, 2048], P(('ep', 'tp')), may hold values from -6 to 6
- moe_gain: float32 [2048], replicated, may hold values from 0.1 to 1.9
- expert_pick: int32 [16384, 2], P(('ep', 'tp')), may hold values from 0 to 31, as said below
- route_weight: float32 [16384, 2], P(('ep', 'tp')), may hold values from 0.1 to 1
- w_gate: bfloat16 [32, 2048, 1024], P('ep', None, 'tp'), may hold values from -0.125 to 0.125
- w_up: bfloat16 [32, 2048, 1024], P('ep', None, 'tp'), may hold values from -0.125 to 0.125
- w_down: bfloat16 [32, 1024, 2048], P('ep', 'tp'), may hold values from -0.1875 to 0.1875
Outputs:
- mixer_out: bfloat16 [16384, 2048], P(('ep', 'tp'))
- routed_out: bfloat16 [16384, 2048], P(('ep', 'tp'))
Inputs may be any that keep to these rules, and one draw needn't show every extreme that they name: `expert_pick`: each row names two different experts of one group, expert e belonging to group e // 8; the rows of one device name no expert more than 16 times, and in every draw each expert of some group is named exactly 16 times by the rows of every device.
All inputs are finite; a program needn't handle non-finite values.
Results may differ from a plain program's by a relative error of at most 0.013.
Values may be sent and summed in bfloat16 or wider, within the bound.
A program may use at most 128 MiB of HBM per device.

v0:
```python
import jax
import jax.numpy as jnp
from jax import lax
from jax.sharding import PartitionSpec as P

HEAD_DIM = 64
GROUPS = 4
TOPK = 2
SEQS = 1


norm_eps = 1e-06


def split_up(value, dim, size):
    lengths = value.shape
    pieces = value.reshape(*lengths[:dim], size, lengths[dim] // size, *lengths[dim + 1 :])
    return jnp.moveaxis(pieces, dim, 0)


def summed_on_arrival(value, axis, dim):
    pieces = split_up(value, dim, lax.axis_size(axis))
    arrived = lax.all_to_all(pieces, axis, split_axis=0, concat_axis=0, tiled=True)
    return arrived.astype(jnp.float32).sum(axis=0)


def gather_turned(arrays, axis, dims):
    turned = [jnp.moveaxis(a, dim, 0) for a, dim in zip(arrays, dims)]
    both = jnp.concatenate([t.reshape(len(t), -1) for t in turned], axis=1)
    filled, at, done = (lax.all_gather(both, axis, axis=0, tiled=True), 0, [])
    for t, dim in zip(turned, dims):
        slab = filled[:, at : at + t[0].size].reshape(-1, *t.shape[1:])
        done.append(jnp.moveaxis(slab, 0, dim))
        at += t[0].size
    return tuple(done)


def block_scores(query_grid, query_pos, key_block, bias_block, key_first):
    key_count = key_block.shape[0]
    head_count = query_grid.shape[1]
    head_width = query_grid.shape[2]
    key_grid = key_block.reshape(key_count, head_count, head_width)
    scores = jnp.einsum("qhd,khd->hqk", query_grid, key_grid, preferred_element_type=jnp.float32)
    scores = scores * head_width ** (-0.5) + jnp.transpose(bias_block)[:, None, :]
    key_pos = key_first + jnp.arange(key_count, dtype=jnp.int32)
    causal = (key_pos[None, :] < query_pos[:, None])[None]
    failure = jnp.where(causal, jax.nn.log_sigmoid(-scores), 0.0)
    return (scores, causal, failure)


def block_values(query_grid, query_pos, key_block, value_block, bias_block, key_first, running):
    scores, causal, failure = block_scores(query_grid, query_pos, key_block, bias_block, key_first)
    remainder = lax.cumsum(failure, axis=2, reverse=True) - failure + running[:, :, None]
    stick_weight = jnp.where(causal, jnp.exp(jax.nn.log_sigmoid(scores) + remainder), 0.0).astype(
        jnp.bfloat16
    )
    value_grid = value_block.reshape(value_block.shape[0], query_grid.shape[1], query_grid.shape[2])
    portion = jnp.einsum(
        "hqk,khd->hqd", stick_weight, value_grid, preferred_element_type=jnp.float32
    )
    return (portion, running + jnp.sum(failure, axis=2))


def held_attend(
    query_grid, query_pos, top_block, seq_base, all_keys, all_values, key_bias, block_rows
):
    row_count = query_grid.shape[0]
    head_count = query_grid.shape[1]
    zero_sum = jnp.zeros((head_count, row_count, query_grid.shape[2]), jnp.float32)
    zero_run = jnp.zeros((head_count, row_count), jnp.float32)

    def visit(step_index, carried):
        key_first = (top_block - step_index) * block_rows
        portion, running = block_values(
            query_grid,
            query_pos,
            lax.dynamic_slice_in_dim(all_keys, key_first, block_rows, 0),
            lax.dynamic_slice_in_dim(all_values, key_first, block_rows, 0),
            lax.dynamic_slice_in_dim(key_bias, key_first, block_rows, 0),
            key_first,
            carried[1],
        )
        return (carried[0] + portion, running)

    return lax.fori_loop(0, top_block - seq_base + 1, visit, (zero_sum, zero_run))[0]


def expand(arrived, gate_weights, up_weights):
    gate_in = jnp.einsum(
        "necm,emf->necf", arrived, gate_weights, preferred_element_type=jnp.float32
    )
    up_in = jnp.einsum("necm,emf->necf", arrived, up_weights, preferred_element_type=jnp.float32)
    return (jax.nn.silu(gate_in) * up_in).astype(jnp.bfloat16)


def contract(hidden, down_weights):
    return jnp.einsum("necf,efm->necm", hidden, down_weights, preferred_element_type=jnp.float32)


def local(
    query_rows,
    key_rows,
    value_rows,
    key_bias,
    out_weight,
    moe_input,
    moe_gain,
    expert_pick,
    route_weight,
    w_gate,
    w_up,
    w_down,
):
    block_rows = query_rows.shape[0]
    half_rows = block_rows // 2
    local_heads = query_rows.shape[1] // HEAD_DIM
    ep_index = lax.axis_index("ep")
    ep_count = lax.axis_size("ep")
    seq_blocks = ep_count // SEQS
    seq_base = ep_index // seq_blocks * seq_blocks
    first_pos = ep_index * block_rows + jnp.arange(half_rows, dtype=jnp.int32)
    second_pos = ep_index * block_rows + half_rows + jnp.arange(half_rows, dtype=jnp.int32)
    query_pos = jnp.concatenate([first_pos, second_pos], axis=0)
    query_grid = query_rows.reshape(block_rows, local_heads, HEAD_DIM)
    all_keys, all_values = (
        lax.all_gather(key_rows, "ep", axis=0, tiled=True),
        lax.all_gather(value_rows, "ep", axis=0, tiled=True),
    )
    attended_sum = held_attend(
        query_grid, query_pos, ep_index, seq_base, all_keys, all_values, key_bias, block_rows
    )
    attended = attended_sum.astype(jnp.bfloat16)
    out_heads = out_weight.reshape(local_heads, HEAD_DIM, out_weight.shape[1])
    chosen = attended
    mixer_out = summed_on_arrival(
        jnp.einsum("hqd,hdm->qm", chosen, out_heads, preferred_element_type=jnp.float32).astype(
            jnp.bfloat16
        ),
        "tp",
        0,
    ).astype(jnp.bfloat16)
    token_count = moe_input.shape[0]
    widened = moe_input.astype(jnp.float32)
    normed = (
        widened
        * lax.rsqrt(jnp.mean(widened * widened, axis=1, keepdims=True) + norm_eps)
        * moe_gain
    ).astype(jnp.bfloat16)
    local_experts = w_gate.shape[0]
    expert_total = local_experts * ep_count
    capacity = GROUPS * token_count // expert_total
    picks = expert_pick.reshape(-1)
    matches = (picks[:, None] == jnp.arange(expert_total, dtype=jnp.int32)[None, :]).astype(
        jnp.int32
    )
    ranks = jnp.sum((jnp.cumsum(matches, axis=0) - matches) * matches, axis=1)
    slots = picks * capacity + ranks
    owners = jnp.arange(picks.shape[0], dtype=jnp.int32) // TOPK
    table = jnp.full((expert_total * capacity,), token_count, jnp.int32).at[slots].set(owners)
    padded = jnp.concatenate([normed, jnp.zeros((1, normed.shape[1]), jnp.bfloat16)], axis=0)
    outgoing = padded[table].reshape(ep_count, local_experts, capacity, normed.shape[1])
    arrived = lax.all_to_all(outgoing, "ep", split_axis=0, concat_axis=0, tiled=True)
    gate_all, up_all, down_all = gather_turned((w_gate, w_up, w_down), "tp", (2, 2, 1))
    served = contract(expand(arrived, gate_all, up_all), down_all).astype(jnp.bfloat16)
    returned = lax.all_to_all(served, "ep", split_axis=0, concat_axis=0, tiled=True)
    flat = returned.reshape(expert_total * capacity, returned.shape[3])
    chosen = flat[slots].reshape(token_count, TOPK, flat.shape[1]).astype(jnp.float32)
    routed_out = jnp.sum(chosen * route_weight[:, :, None], axis=1).astype(jnp.bfloat16)
    return (mixer_out, routed_out)


def solution(mesh):
    placed = (
        P("ep", "tp"),
        P("ep", "tp"),
        P("ep", "tp"),
        P(None, "tp"),
        P("tp", None),
        P(("ep", "tp"), None),
        P(),
        P(("ep", "tp"), None),
        P(("ep", "tp"), None),
        P("ep", None, "tp"),
        P("ep", None, "tp"),
        P("ep", "tp", None),
    )
    return jax.shard_map(
        local,
        mesh=mesh,
        in_specs=placed,
        out_specs=(P(("ep", "tp"), None), P(("ep", "tp"), None)),
        check_vma=False,
    )
```

profile of v0, /device:TPU:1, one launch (start us, length us, event | category | flops | bytes accessed | tf_op | source)
XLA Modules:
  0.0 1562.6 jit_solution(7733374243366959286)
XLA Ops:
  12.6 3.1 pad_maximum_fusion
  19.2 3.3 gather_fusion
  22.5 9.8 all-to-all-start.1
  32.5 54.7 %all-gather.4.cloned.1.call-done = bf16[16384,256]{0,1:T(8,128)(2,1)} async-done(((bf16[512,256]{0,1:T(8,128)(2,1)}), bf16[16384,256]{0,1:T(8,128)(2,1)}) %all-gather.4.cloned.1.call-update) | async-done | bytes 8388624 | tf_op jit(solution)/shard_map/all_gather | solution.py:126
  87.2 61.3 %all-gather.6.cloned.1.call-done = bf16[16384,256]{0,1:T(8,128)(2,1)} async-done(((bf16[512,256]{0,1:T(8,128)(2,1)}), bf16[16384,256]{0,1:T(8,128)(2,1)}) %all-gather.6.cloned.1.call-update) | async-done | bytes 8388624 | tf_op jit(solution)/shard_map/all_gather | solution.py:127
  148.6 108.0 %while.12 = (s32[]{:T(128)}, f32[4,512,64]{1,2,0:T(8,128)S(1)}, f32[4,512]{1,0:T(4,128)S(1)}, s32[]{:T(128)}, s32[]{:T(128)}, /*index=5*/s32[512]{0:T(512)S(1)},...) while((s32[]{:T(128)}, f32[4,512,64]{1,2,0:T(8,128)S(1)}, ...), condition=%wide.region_4.5_spmd, body=%wide.region_0.4_spmd.sunk | while | flops 438729216 | bytes 83679512 | solution.py:85
  169.8 5.1 fusion.66
  174.9 19.4 %fusion.67 = f32[4,512,4,128]{1,2,3,0:T(4,128)S(1)} fusion(f32[4,512,4,128]{1,3,2,0:T(8,128)S(1)} %bitcast.193), kind=kOutput, calls=%fused_computation.21.clone.1 | output fusion | flops 133169152 | bytes 8388608 | tf_op jit(solution)/shard_map/reduce-window
  196.4 2.9 broadcast_add_fusion.2
  201.6 6.7 fusion.68
  210.8 5.1 fusion.66
  215.9 19.4 %fusion.67 = f32[4,512,4,128]{1,2,3,0:T(4,128)S(1)} fusion(f32[4,512,4,128]{1,3,2,0:T(8,128)S(1)} %bitcast.193), kind=kOutput, calls=%fused_computation.21.clone.1 | output fusion | flops 133169152 | bytes 8388608 | tf_op jit(solution)/shard_map/reduce-window
  237.4 2.9 broadcast_add_fusion.2
  242.6 6.7 fusion.68
  258.7 4.1 all-to-all-start
  262.8 24.4 %all-gather.8.cloned.1.call-done = bf16[1024,6144]{0,1:T(8,128)(2,1)} async-done(((bf16[256,6144]{0,1:T(8,128)(2,1)}), bf16[1024,6144]{0,1:T(8,128)(2,1)}) %all-gather.8.cloned.1.call-update) | async-done | bytes 12582928 | tf_op jit(solution)/shard_map/all_gather | solution.py:30
  287.2 6.7 fusion.15
  293.9 11.0 fusion.19
  304.8 4.1 copy.52
  310.2 1208.4 %all-to-all-start.2 = ((bf16[32,1,16,2048]{3,2,1,0:T(8,128)(2,1)}), bf16[32,1,16,2048]{3,2,1,0:T(8,128)(2,1)S(1)}, u32[]{:S(2)}, u32[]{:S(2)}) async-start(bf16[32,1,16,2048]{3,2,1,0:T(8,128)(2,1)} %copy.52), calls=%async_computation.2 | async-start | bytes 4194304 | tf_op jit(solution)/shard_map/all_to_all | solution.py:165
  1518.8 2.9 reduce_sum.50
  1521.7 25.5 %all-to-all-done.2 = bf16[32,1,16,2048]{3,2,1,0:T(8,128)(2,1)S(1)} async-done(((bf16[32,1,16,2048]{3,2,1,0:T(8,128)(2,1)}), bf16[32,1,16,2048]{3,2,1,0:T(8,128)(2,1)S(1)}, u32[]{:S(2)}, u32[]{:S(2)}) %all-to-all-start.2) | async-done | bytes 2097184 | tf_op jit(solution)/shard_map/all_to_all | solution.py:165
  1549.5 2.4 reshape.171
  1551.9 3.9 multiply_reduce_fusion
  (83 shorter events, 28.6 us)
Async XLA Ops:
  7.2 249.4 %copy-start = (bf16[256,2048]{1,0:T(8,128)(2,1)S(1)}, bf16[256,2048]{1,0:T(8,128)(2,1)}, u32[]{:S(2)}) copy-start(bf16[256,2048]{1,0:T(8,128)(2,1)} %param.18) | copy-start | bytes 3145732
  7.2 80.0 %all-gather.4.cloned.1.call-start = ((), (), s32[]{:S(2)}) async-start(), calls=%async_computation.3 | async-start | bytes 8650752 | tf_op jit(solution)/shard_map/all_gather | solution.py:126
  9.1 139.4 %all-gather.6.cloned.1.call-start = ((), (), s32[]{:S(2)}) async-start(), calls=%async_computation.4 | async-start | bytes 8650752 | tf_op jit(solution)/shard_map/all_gather | solution.py:127
  11.0 276.2 %all-gather.8.cloned.1.call-start = ((), (), s32[]{:S(2)}) async-start(), calls=%async_computation.5 | async-start | bytes 15728640 | tf_op jit(solution)/shard_map/all_gather | solution.py:30
  12.5 3.1 copy-start.7
  12.5 4.6 copy-start.4
  12.6 4.8 copy-start.6
  22.5 9.8 copy-start.5
  22.5 236.2 %all-to-all-start.1 = ((bf16[32,1,16,2048]{3,2,1,0:T(8,128)(2,1)}), bf16[32,1,16,2048]{3,2,1,0:T(8,128)(2,1)}, u32[]{:S(2)}, u32[]{:S(2)}) async-start(bf16[32,1,16,2048]{3,2,1,0:T(8,128)(2,1)} %bitcast.196), calls=%async_computation.1 | async-start | bytes 4194304 | tf_op jit(solution)/shard_map/all_to_all | solution.py:162
  194.3 2.0 copy-start.1
  199.3 2.2 copy-start.2
  235.2 2.0 copy-start.1
  240.3 2.3 copy-start.2
  258.7 50.2 %all-to-all-start = ((bf16[4,128,2048]{2,1,0:T(8,128)(2,1)}), bf16[4,128,2048]{2,1,0:T(8,128)(2,1)S(1)}, u32[]{:S(2)}, u32[]{:S(2)}) async-start(bf16[4,128,2048]{2,1,0:T(8,128)(2,1)} %bitcast.199), calls=%async_computation | async-start | bytes 4194304 | tf_op jit(solution)/shard_map/all_to_all | solution.py:23
  304.8 1213.8 %copy-start.8 = (f32[128,2]{0,1:T(2,128)S(1)}, f32[128,2]{0,1:T(2,128)}, u32[]{:S(2)}) copy-start(f32[128,2]{0,1:T(2,128)} %param.22) | copy-start | bytes 3076
  308.9 1.3 copy-start.3
  310.2 1237.0 %all-to-all-start.2 = ((bf16[32,1,16,2048]{3,2,1,0:T(8,128)(2,1)}), bf16[32,1,16,2048]{3,2,1,0:T(8,128)(2,1)S(1)}, u32[]{:S(2)}, u32[]{:S(2)}) async-start(bf16[32,1,16,2048]{3,2,1,0:T(8,128)(2,1)} %copy.52), calls=%async_computation.2 | async-start | bytes 4194304 | tf_op jit(solution)/shard_map/all_to_all | solution.py:165
Sparse Core Ops, SparseCore 0:
  10.7 76.4 all-gather.3
  90.0 58.5 all-gather.5
  150.2 136.9 all-gather.7
where the time goes:
time: 1570 us; the launch traced here: 1560 us
  starting transfers between devices  1220 us (78%)
  waiting for transfers between devices  166 us (11%)
  other arithmetic  69.6 us (4%)
  local copies, waits for them, and re-layouts  33.3 us (2%)
  matrix products  30.9 us (2%)
  loops' own time  26.2 us (2%)
    all_to_all x1, starting transfers between devices, local(): lax.all_to_all(served, 'ep', split_axis=0, concat_axis=0, tiled=True)  1210 us
    all_gather x1, waiting for transfers between devices, local(): lax.all_gather(value_rows, 'ep', axis=0, tiled=True)  61.3 us
    all_gather x1, waiting for transfers between devices, local(): lax.all_gather(key_rows, 'ep', axis=0, tiled=True)  54.7 us
    another operation x6, other arithmetic  39.5 us
  transfers between devices with their start and end apart: 6, of which 4 were waited for; matrix products, arithmetic and copies ran while one was open for 7% of the time, Pallas kernels for 0%

commit v1 on v0

v1 whole, which is shorter than its diff:
```python
import math

import jax
import jax.numpy as jnp
from jax import lax
from jax.experimental import pallas as pl
from jax.experimental.pallas import tpu as pltpu
from jax.sharding import PartitionSpec as P

HEAD_DIM = 64
GROUPS = 4
TOPK = 2
BLOCK = 512
HALF = 256
RUNS = 8
RUN = HALF // RUNS
LOG2E = math.log2(math.e)
U_CAP = 48.0
norm_eps = 1e-06


def attend_kernel(tiles_ref, qt_ref, kv_ref, bias_ref, out_ref, kk_ref, rhs_ref, z_hi, z_lo, w_hi, w_lo, acc_ref, carry_ref):
    lanes = qt_ref.shape[2]
    low_lane = lax.broadcasted_iota(jnp.int32, (HALF, 128), 1) < HEAD_DIM
    sub = lax.broadcasted_iota(jnp.int32, (RUNS, 128), 0)
    row = lax.broadcasted_iota(jnp.int32, (128, lanes), 0)

    def build(b, carried):
        pair = kv_ref[b, 0:HALF, :].astype(jnp.float32)
        turned = pltpu.roll(pair, HEAD_DIM, axis=1)
        kk_ref[b, 0] = jnp.where(low_lane, pair, turned).astype(jnp.bfloat16)
        kk_ref[b, 1] = jnp.where(low_lane, turned, pair).astype(jnp.bfloat16)
        return carried

    lax.fori_loop(0, kv_ref.shape[0], build, 0)

    def later(x, n):
        return jnp.where(sub < RUNS - n, pltpu.roll(x, RUNS - n, axis=0), 1.0)

    def scores(b, half, z_ref):
        keys = jnp.concatenate([kk_ref[b, half], bias_ref[b, half]], axis=1)
        z_ref[...] = jnp.dot(keys, rhs_ref[...], preferred_element_type=jnp.float32)

    def weigh(z_ref, w_ref, first_key):
        for lane in range(0, lanes, 128):
            ls = slice(lane, lane + 128)
            us = []
            for i in range(RUN):
                u = jnp.exp2(jnp.minimum(z_ref[RUNS * i : RUNS * i + RUNS, ls], U_CAP))
                if first_key is not None:
                    query = lax.broadcasted_iota(jnp.int32, (RUNS, 128), 1) + lane
                    u = jnp.where(sub * RUN + (i + first_key) < query, u, 0.0)
                us.append(u)
            pairs = range(RUN // 2)
            rs = [1.0 / ((1.0 + us[2 * g]) * (1.0 + us[2 * g + 1])) for g in pairs]
            tree = list(rs)
            while len(tree) > 1:
                tree = [tree[2 * n] * tree[2 * n + 1] for n in range(len(tree) // 2)]
            total = tree[0]
            after = later(total, 1)
            after = after * later(after, 1)
            after = after * later(after, 2)
            after = after * later(after, 4)
            carry = carry_ref[:, ls]
            left = carry * after
            carry_ref[:, ls] = carry * jnp.broadcast_to((after * total)[0:1, :], (RUNS, 128))
            for g in reversed(pairs):
                left = left * rs[g]
                first = us[2 * g] * left
                second = us[2 * g + 1] * (left * (1.0 + us[2 * g]))
                both = jnp.concatenate([first, second], axis=0)
                w_ref[2 * RUNS * g : 2 * RUNS * g + 2 * RUNS, ls] = both.astype(jnp.bfloat16)

    def collect(b, half, w_ref):
        at = HALF + 2 * HEAD_DIM * half
        values = jnp.concatenate([kv_ref[b, at : at + HEAD_DIM, :], kv_ref[b, at + HEAD_DIM : at + 2 * HEAD_DIM, :]], axis=1)
        acc_ref[...] += jnp.dot(values, w_ref[...], preferred_element_type=jnp.float32)

    def tile(n, carried):
        p = tiles_ref[n]
        scaled = qt_ref[n].astype(jnp.float32) * (LOG2E * HEAD_DIM**-0.5)
        top = scaled.astype(jnp.bfloat16)
        rhs_ref[0:HEAD_DIM, :] = top
        rhs_ref[HEAD_DIM : 2 * HEAD_DIM, :] = (scaled - top.astype(jnp.float32)).astype(jnp.bfloat16)
        rhs_ref[128:256, :] = jnp.where(row < 3, 1.0, 0.0).astype(jnp.bfloat16)
        carry_ref[...] = jnp.ones_like(carry_ref)
        acc_ref[...] = jnp.zeros_like(acc_ref)
        scores(p, 1, z_hi)
        scores(p, 0, z_lo)
        weigh(z_hi, w_hi, HALF)
        scores(jnp.maximum(p - 1, 0), 1, z_hi)
        weigh(z_lo, w_lo, 0)
        collect(p, 1, w_hi)

        def visit(step, inner):
            b = p - 1 - step
            scores(b, 0, z_lo)
            weigh(z_hi, w_hi, None)
            collect(b + 1, 0, w_lo)
            scores(jnp.maximum(b - 1, 0), 1, z_hi)
            weigh(z_lo, w_lo, None)
            collect(b, 1, w_hi)
            return inner

        lax.fori_loop(0, p, visit, 0)
        collect(0, 0, w_lo)
        out_ref[n] = acc_ref[...].astype(jnp.bfloat16)
        return carried

    lax.fori_loop(0, qt_ref.shape[0], tile, 0)


def attend(tiles, qt, kv, bias):
    n_tiles, width, lanes = qt.shape
    blocks = kv.shape[0]
    whole = pl.BlockSpec(memory_space=pltpu.VMEM)
    return pl.pallas_call(
        attend_kernel,
        out_shape=jax.ShapeDtypeStruct((n_tiles, width, lanes), jnp.bfloat16),
        in_specs=[pl.BlockSpec(memory_space=pltpu.SMEM), whole, whole, whole],
        out_specs=whole,
        scratch_shapes=[
            pltpu.VMEM((blocks, 2, HALF, 128), jnp.bfloat16),
            pltpu.VMEM((HALF, lanes), jnp.bfloat16),
            pltpu.VMEM((HALF, lanes), jnp.float32),
            pltpu.VMEM((HALF, lanes), jnp.float32),
            pltpu.VMEM((HALF, lanes), jnp.bfloat16),
            pltpu.VMEM((HALF, lanes), jnp.bfloat16),
            pltpu.VMEM((width, lanes), jnp.float32),
            pltpu.VMEM((RUNS, lanes), jnp.float32),
        ],
        cost_estimate=pl.CostEstimate(flops=40_000_000_000, bytes_accessed=12 << 20, transcendentals=0),
        name="stick_attend",
    )(tiles, qt, kv, bias)


def key_order(rows):
    n = rows.shape[-1]
    return rows.reshape(2, RUNS, RUN, n).swapaxes(1, 2).reshape(BLOCK, n)


def bias_lanes(bias):
    left = bias * LOG2E
    lane = lax.broadcasted_iota(jnp.int32, bias.shape[:3] + (128,), 3)
    out = jnp.zeros(lane.shape, jnp.float32)
    for n in range(3):
        part = lax.reduce_precision(left, 8, 7)
        out = jnp.where(lane == n, part, out)
        left = left - part
    return out.astype(jnp.bfloat16)


def slot_and_turn(block):
    slot, at = block // 8, block % 8
    return slot, at if slot % 2 == 0 else 7 - at


def routes(turn):
    pairs = []
    for block in range(32):
        slot, j = slot_and_turn(block)
        pairs.append((block, j // 2 * 8 + (slot + turn) % 4 * 2 + j % 2))
    return pairs


def mixer(query_rows, key_rows, value_rows, key_bias, out_weight):
    ep_index = lax.axis_index("ep")
    head = ep_index // 2 % 4
    turn = ep_index // 8 * 2 + ep_index % 2
    my_slot = ep_index // 8

    q_heads = query_rows.T.reshape(4, HEAD_DIM, BLOCK)
    keys = key_order(key_rows).reshape(2, HALF, 4, HEAD_DIM)
    k_heads = keys.transpose(2, 1, 0, 3).reshape(4, HALF, 128)
    values = key_order(value_rows).T.reshape(4, HEAD_DIM, 4, 128)
    v_heads = values.transpose(0, 2, 1, 3).reshape(4, HALF, 128)
    kv_heads = jnp.concatenate([k_heads, v_heads], axis=1)
    kv_out = jnp.broadcast_to(kv_heads[None, :, None], (4, 4, 2, BLOCK, 128)).reshape(32, BLOCK, 128)
    kv = lax.all_to_all(kv_out, "ep", split_axis=0, concat_axis=0, tiled=True)

    q_twice = jnp.concatenate([q_heads, q_heads], axis=0)
    q_got, tiles = [], []
    for r in range(4):
        mine = lax.dynamic_index_in_dim(q_twice, my_slot + r, 0, keepdims=False)
        q_got.append(lax.ppermute(mine, "ep", routes(r)))
        slot = (head - r + 4) % 4
        tiles.append(slot * 8 + jnp.where(slot % 2 == 0, turn, 7 - turn))
    qt = jnp.stack(q_got)
    tiles = jnp.stack(tiles).astype(jnp.int32)

    column = lax.dynamic_slice_in_dim(key_bias, head, 1, 1)
    bias = bias_lanes(column.reshape(32, 2, RUNS, RUN, 1).swapaxes(2, 3).reshape(32, 2, HALF, 1))

    done = attend(tiles, qt, kv, bias)

    back = [lax.ppermute(done[r], "ep", [(b, a) for a, b in routes(r)]) for r in range(4)]
    twice = jnp.stack(back + back)
    attended = lax.dynamic_slice_in_dim(twice, 4 - my_slot, 4, 0)
    pieces = attended.reshape(4 * HEAD_DIM, 4, 128).swapaxes(0, 1)
    columns = lax.all_to_all(pieces, "tp", split_axis=0, concat_axis=0, tiled=True)
    weight = lax.all_gather(out_weight, "tp", axis=0, tiled=True)
    columns = columns.reshape(weight.shape[0], 128)
    return jnp.einsum("cr,cm->rm", columns, weight, preferred_element_type=jnp.float32).astype(jnp.bfloat16)


def gather_turned(arrays, axis, dims):
    turned = [jnp.moveaxis(a, dim, 0) for a, dim in zip(arrays, dims)]
    both = jnp.concatenate([t.reshape(len(t), -1) for t in turned], axis=1)
    filled, at, done = (lax.all_gather(both, axis, axis=0, tiled=True), 0, [])
    for t, dim in zip(turned, dims):
        slab = filled[:, at : at + t[0].size].reshape(-1, *t.shape[1:])
        done.append(jnp.moveaxis(slab, 0, dim))
        at += t[0].size
    return tuple(done)


def expand(arrived, gate_weights, up_weights):
    gate_in = jnp.einsum("necm,emf->necf", arrived, gate_weights, preferred_element_type=jnp.float32)
    up_in = jnp.einsum("necm,emf->necf", arrived, up_weights, preferred_element_type=jnp.float32)
    return (jax.nn.silu(gate_in) * up_in).astype(jnp.bfloat16)


def contract(hidden, down_weights):
    return jnp.einsum("necf,efm->necm", hidden, down_weights, preferred_element_type=jnp.float32)


def experts(moe_input, moe_gain, expert_pick, route_weight, w_gate, w_up, w_down):
    ep_count = lax.axis_size("ep")
    token_count = moe_input.shape[0]
    widened = moe_input.astype(jnp.float32)
    normed = (
        widened * lax.rsqrt(jnp.mean(widened * widened, axis=1, keepdims=True) + norm_eps) * moe_gain
    ).astype(jnp.bfloat16)
    local_experts = w_gate.shape[0]
    expert_total = local_experts * ep_count
    capacity = GROUPS * token_count // expert_total
    picks = expert_pick.reshape(-1)
    matches = (picks[:, None] == jnp.arange(expert_total, dtype=jnp.int32)[None, :]).astype(jnp.int32)
    ranks = jnp.sum((jnp.cumsum(matches, axis=0) - matches) * matches, axis=1)
    slots = picks * capacity + ranks
    owners = jnp.arange(picks.shape[0], dtype=jnp.int32) // TOPK
    table = jnp.full((expert_total * capacity,), token_count, jnp.int32).at[slots].set(owners)
    padded = jnp.concatenate([normed, jnp.zeros((1, normed.shape[1]), jnp.bfloat16)], axis=0)
    outgoing = padded[table].reshape(ep_count, local_experts, capacity, normed.shape[1])
    arrived = lax.all_to_all(outgoing, "ep", split_axis=0, concat_axis=0, tiled=True)
    gate_all, up_all, down_all = gather_turned((w_gate, w_up, w_down), "tp", (2, 2, 1))
    served = contract(expand(arrived, gate_all, up_all), down_all).astype(jnp.bfloat16)
    returned = lax.all_to_all(served, "ep", split_axis=0, concat_axis=0, tiled=True)
    flat = returned.reshape(expert_total * capacity, returned.shape[3])
    chosen = flat[slots].reshape(token_count, TOPK, flat.shape[1]).astype(jnp.float32)
    return jnp.sum(chosen * route_weight[:, :, None], axis=1).astype(jnp.bfloat16)


def local(
    query_rows, key_rows, value_rows, key_bias, out_weight, moe_input, moe_gain,
    expert_pick, route_weight, w_gate, w_up, w_down,
):
    routed_out = experts(moe_input, moe_gain, expert_pick, route_weight, w_gate, w_up, w_down)
    mixer_out = mixer(query_rows, key_rows, value_rows, key_bias, out_weight)
    return (mixer_out, routed_out)


def solution(mesh):
    placed = (
        P("ep", "tp"), P("ep", "tp"), P("ep", "tp"), P(None, "tp"), P("tp", None),
        P(("ep", "tp"), None), P(), P(("ep", "tp"), None), P(("ep", "tp"), None),
        P("ep", None, "tp"), P("ep", None, "tp"), P("ep", "tp", None),
    )
    return jax.shard_map(
        local,
        mesh=mesh,
        in_specs=placed,
        out_specs=(P(("ep", "tp"), None), P(("ep", "tp"), None)),
        check_vma=False,
    )
```

time: 1570 us -> 225 us (0.14)
  starting transfers between devices: 1220 us -> 48.5 us
  waiting for transfers between devices: 166 us -> 54.4 us
  other arithmetic: 69.6 us -> 19.5 us
  Pallas kernels: 0 us -> 44.5 us
  loops' own time: 26.2 us -> 0 us
    all_to_all x3 -> x4, starting transfers between devices: 1220 us -> 31.2 us  [the longest x1 9.78 us: mixer(): kv = lax.all_to_all(kv_out, 'ep', split_axis=0, concat_axis=0, tiled=True)]
    all_gather x2 -> x1, waiting for transfers between devices: 116 us -> 8.64 us  [mixer(): weight = lax.all_gather(out_weight, 'tp', axis=0, tiled=True)]
    pallas_call x0 -> x1, Pallas kernels: none -> 44.5 us  [attend(): pl.pallas_call(attend_kernel, out_shape=jax.ShapeDtypeStruct((n_tiles, wi...]
    another operation x8 -> x4, other arithmetic: 45.4 us -> 2.04 us  [the longest x1 0.74 us: mixer(): qt = jnp.stack(q_got)]
    ppermute x0 -> x8, waiting for transfers between devices: none -> 29.7 us  [the longest x4 23.7 us: mixer(): q_got.append(lax.ppermute(mine, 'ep', routes(r)))]
    another operation x1 -> x0, loops' own time: 26.2 us -> none  [held_attend(): lax.fori_loop(0, top_block - seq_base + 1, visit, (zero_sum, zero_run))[0]]
    all_gather x1, waiting for transfers between devices: 24.4 us -> 0.01 us  [gather_turned(): filled, at, done = (lax.all_gather(both, axis, axis=0, tiled=True), 0, [])]
    ppermute x0 -> x8, starting transfers between devices: none -> 17.2 us  [the longest x4 8.85 us: mixer(): q_got.append(lax.ppermute(mine, 'ep', routes(r)))]
  transfers between devices with their start and end apart: 6 -> 14, of which waited for: 4 -> 8; matrix products, arithmetic and copies ran while one was open for 7% -> 22% of each run, Pallas kernels for 0% -> 20%
where the time goes in v1:
time: 225 us; the launch traced here: 224 us
  waiting for transfers between devices  54.4 us (24%)
  starting transfers between devices  48.5 us (22%)
  Pallas kernels  44.5 us (20%)
  local copies, waits for them, and re-layouts  21.9 us (10%)
  matrix products  20.2 us (9%)
  other arithmetic  19.5 us (9%)
  between operations  14.6 us (6%)
    pallas_call x1, Pallas kernels, attend(): pl.pallas_call(attend_kernel, out_shape=jax.ShapeDtypeStruct((n_tiles, wi...  44.5 us
    ppermute x4, waiting for transfers between devices, mixer(): q_got.append(lax.ppermute(mine, 'ep', routes(r)))  23.7 us
    all_to_all x1, waiting for transfers between devices, experts(): lax.all_to_all(served, 'ep', split_axis=0, concat_axis=0, tiled=True)  16 us
    dot_general x1, matrix products, contract(): jnp.einsum('necf,efm->necm', hidden, down_weights, preferred_element_type...  10.4 us
    all_to_all x1, starting transfers between devices, mixer(): kv = lax.all_to_all(kv_out, 'ep', split_axis=0, concat_axis=0, tiled=True)  9.78 us
    all_to_all x1, starting transfers between devices, experts(): lax.all_to_all(outgoing, 'ep', split_axis=0, concat_axis=0, tiled=True)  8.97 us
    ppermute x4, starting transfers between devices, mixer(): q_got.append(lax.ppermute(mine, 'ep', routes(r)))  8.85 us
    all_gather x1, waiting for transfers between devices, mixer(): weight = lax.all_gather(out_weight, 'tp', axis=0, tiled=True)  8.64 us
  transfers between devices with their start and end apart: 14, of which 8 were waited for; matrix products, arithmetic and copies ran while one was open for 22% of the time, Pallas kernels for 20%

profile of v1, /device:TPU:1, one launch (start us, length us, event | category | flops | bytes accessed | tf_op | source)
XLA Modules:
  0.0 223.5 jit_solution(10104041784231770280)
XLA Ops:
  8.7 3.0 %pad_maximum_fusion = bf16[256,6144]{0,1:T(8,128)(2,1)} fusion(bf16[256,2048]{0,1:T(8,128)(2,1)S(1)} %bitcast.187, bf16[256,2048]{0,1:T(8,128)(2,1)} %bitcast.198, bf16[256,2048]{0,1:T(8,128)(2,1)} %bitcast.199), kind=kLoop, calls=%fused_computation.10 | loop fusion | flops 9437184 | bytes 6291456 | tf_op jit(solution)/shard_map/concatenate | solution.py:208
  14.3 2.9 %broadcast_in_dim.40 = bf16[4,4,2,512,128]{4,3,2,1,0:T(8,128)(2,1)} broadcast(bf16[4,512,128]{2,1,0:T(8,128)(2,1)S(1)} %copy.91), dimensions={1,3,4} | broadcast | bytes 4718592 | tf_op jit(solution)/shard_map/broadcast_in_dim | solution.py:178
  17.2 9.8 %all-to-all-start = ((bf16[32,512,128]{2,1,0:T(8,128)(2,1)}), bf16[32,512,128]{2,1,0:T(8,128)(2,1)}, u32[]{:S(2)}, u32[]{:S(2)}) async-start(bf16[32,512,128]{2,1,0:T(8,128)(2,1)} %bitcast.186), calls=%async_computation | async-start | bytes 8388608 | tf_op jit(solution)/shard_map/all_to_all | solution.py:179
  27.4 2.9 %collective-permute-start.2 = (bf16[64,512]{1,0:T(8,128)(2,1)S(1)}, bf16[64,512]{1,0:T(8,128)(2,1)S(1)}, u32[]{:S(2)}, u32[]{:S(2)}) collective-permute-start(bf16[64,512]{1,0:T(8,128)(2,1)S(1)} %get-tuple-element.7), channel_id=1, source_target_pairs={{0,16},{4,20},{8,48},{12,52},{16,80},{20,84},{24,112},{28,116},{32... | collective-permute-start | bytes 196616 | tf_op jit(solution)/shard_map/ppermute | solution.py:185
  30.3 2.5 %collective-permute-start.3 = (bf16[64,512]{1,0:T(8,128)(2,1)S(1)}, bf16[64,512]{1,0:T(8,128)(2,1)S(1)}, u32[]{:S(2)}, u32[]{:S(2)}) collective-permute-start(bf16[64,512]{1,0:T(8,128)(2,1)S(1)} %get-tuple-element.9), channel_id=1, source_target_pairs={{0,24},{4,28},{8,56},{12,60},{16,88},{20,92},{24,120},{28,124},{32... | collective-permute-start | bytes 196616 | tf_op jit(solution)/shard_map/ppermute | solution.py:185
  33.4 2.8 %collective-permute-start.1 = (bf16[64,512]{1,0:T(8,128)(2,1)S(1)}, bf16[64,512]{1,0:T(8,128)(2,1)S(1)}, u32[]{:S(2)}, u32[]{:S(2)}) collective-permute-start(bf16[64,512]{1,0:T(8,128)(2,1)S(1)} %get-tuple-element.8), channel_id=1, source_target_pairs={{0,8},{4,12},{8,40},{12,44},{16,72},{20,76},{24,104},{28,108},{32,... | collective-permute-start | bytes 196616 | tf_op jit(solution)/shard_map/ppermute | solution.py:185
  41.6 3.4 %gather_fusion = bf16[512,2048]{1,0:T(8,128)(2,1)} fusion(bf16[129,2048]{1,0:T(8,128)(2,1)S(1)} %concatenate.15, s32[1024]{0:T(1024)S(1)} %pad_clamp_fusion.1), kind=kCustom, calls=%fused_computation | custom fusion | bytes 4196352 | tf_op jit(solution)/shard_map/gather | solution.py:244
  44.9 8.6 %select_convert_fusion.bias_ref = bf16[32,2,256,128]{3,2,1,0:T(8,128)(2,1)} fusion(bf16[32,2,256]{2,1,0:T(2,128)(2,1)S(1)} %copy.97, bf16[32,2,256]{2,1,0:T(2,128)(2,1)S(1)} %copy.96, bf16[32,2,256]{2,1,0:T(2,128)(2,1)S(1)} %copy.95, pred[128]{0:T(512)(128)(4,1)S(1)} %get-tuple-element.13, pred[128]{0:T(512)(128)(4,1)S(1)} %get-tuple-element.14, ...), kind=kLoop, calls=%fused_computation.3 | loop fusion | flops 6291456 | bytes 4292992 | tf_op jit(solution)/shard_map/convert_element_type | solution.py:150
  54.2 21.2 %collective-permute-done.2 = bf16[64,512]{1,0:T(8,128)(2,1)S(1)} collective-permute-done((bf16[64,512]{1,0:T(8,128)(2,1)S(1)}, bf16[64,512]{1,0:T(8,128)(2,1)S(1)}, u32[]{:S(2)}, u32[]{:S(2)}) %collective-permute-start.2) | collective-permute-done | bytes 65568 | tf_op jit(solution)/shard_map/ppermute | solution.py:185
  76.3 1.7 collective-permute-done.1
  78.7 9.0 %all-to-all-start.2 = ((bf16[32,1,16,2048]{3,2,1,0:T(8,128)(2,1)}), bf16[32,1,16,2048]{3,2,1,0:T(8,128)(2,1)S(1)}, u32[]{:S(2)}, u32[]{:S(2)}) async-start(bf16[32,1,16,2048]{3,2,1,0:T(8,128)(2,1)} %bitcast.52), calls=%async_computation.2 | async-start | bytes 4194304 | tf_op jit(solution)/shard_map/all_to_all | solution.py:245
  87.7 44.5 %stick_attend.1 = bf16[4,64,512]{2,1,0:T(8,128)(2,1)} custom-call(s32[4]{0:T(128)} %pad_add_fusion.tiles_ref, bf16[4,64,512]{2,1,0:T(8,128)(2,1)} %pad_maximum_fusion.2.qt_ref, bf16[32,512,128]{2,1,0:T(8,128)(2,1)} %all-to-all-done.kv_ref, bf16[32,2,256,128]{3,2,1,0:T(8,128)(2,1)} %select_convert_fusion.bias_ref), custom_call_target="tpu_custom_call" | custom-call | flops 40000000000 | bytes 12582912 | tf_op jit(solution)/shard_map/stick_attend/pallas_call | solution.py:117
  133.9 6.6 %collective-permute-start.5 = (bf16[64,512]{1,0:T(8,128)(2,1)S(1)}, bf16[64,512]{1,0:T(8,128)(2,1)S(1)}, u32[]{:S(2)}, u32[]{:S(2)}) collective-permute-start(bf16[64,512]{1,0:T(8,128)(2,1)S(1)} %get-tuple-element.4), channel_id=1, source_target_pairs={{8,0},{12,4},{40,8},{44,12},{72,16},{76,20},{104,24},{108,28},{116... | collective-permute-start | bytes 196616 | tf_op jit(solution)/shard_map/ppermute | solution.py:196
  143.2 2.7 %collective-permute-done.6 = bf16[64,512]{1,0:T(8,128)(2,1)S(1)} collective-permute-done((bf16[64,512]{1,0:T(8,128)(2,1)S(1)}, bf16[64,512]{1,0:T(8,128)(2,1)S(1)}, u32[]{:S(2)}, u32[]{:S(2)}) %collective-permute-start.6) | collective-permute-done | bytes 65568 | tf_op jit(solution)/shard_map/ppermute | solution.py:196
  145.9 1.7 collective-permute-done.7
  148.5 4.0 %all-to-all-start.1 = ((bf16[4,256,128]{2,1,0:T(8,128)(2,1)}), bf16[4,256,128]{2,1,0:T(8,128)(2,1)S(1)}, u32[]{:S(2)}, u32[]{:S(2)}) async-start(bf16[4,256,128]{2,1,0:T(8,128)(2,1)} %copy.98), calls=%async_computation.1 | async-start | bytes 524288 | tf_op jit(solution)/shard_map/all_to_all | solution.py:200
  152.5 6.0 %fusion = f32[1024,32,16]{0,1,2:T(8,128)} fusion(bf16[1024,6144]{0,1:T(8,128)(2,1)} %all-gather.5.cloned.1.call-done, bf16[32,1,16,2048]{3,2,1,0:T(8,128)(2,1)S(1)} %all-to-all-done.2), kind=kOutput, calls=%fused_computation.5 | convolution fusion | flops 2147483648 | bytes 8388608 | tf_op jit(solution)/shard_map/necm,emf->necf/dot_general | solution.py:219
  158.5 10.4 %fusion.4 = bf16[32,1,16,2048]{3,0,2,1:T(8,128)(2,1)} fusion(bf16[1024,6144]{0,1:T(8,128)(2,1)} %all-gather.5.cloned.1.call-done, f32[1024,32,16]{0,1,2:T(8,128)} %fusion, bf16[32,1,16,2048]{3,2,1,0:T(8,128)(2,1)S(1)} %all-to-all-done.2), kind=kOutput, calls=%fused_computation.12 | convolution fusion | flops 4299161600 | bytes 14680064 | tf_op jit(solution)/shard_map/necf,efm->necm/dot_general | solution.py:224
  169.0 4.1 %copy.107 = bf16[32,1,16,2048]{3,2,1,0:T(8,128)(2,1)} copy(bf16[32,1,16,2048]{3,0,2,1:T(8,128)(2,1)} %fusion.4) | data formatting | bytes 4194304 | tf_op jit(solution)/shard_map/convert_element_type | solution.py:247
  173.1 8.5 %all-to-all-start.3 = ((bf16[32,1,16,2048]{3,2,1,0:T(8,128)(2,1)}), bf16[32,1,16,2048]{3,2,1,0:T(8,128)(2,1)S(1)}, u32[]{:S(2)}, u32[]{:S(2)}) async-start(bf16[32,1,16,2048]{3,2,1,0:T(8,128)(2,1)} %copy.107), calls=%async_computation.3 | async-start | bytes 4194304 | tf_op jit(solution)/shard_map/all_to_all | solution.py:248
  181.6 8.6 %all-gather.3.cloned.1.call-done = bf16[1024,2048]{1,0:T(8,128)(2,1)} async-done(((bf16[256,2048]{1,0:T(8,128)(2,1)}), bf16[1024,2048]{1,0:T(8,128)(2,1)}) %all-gather.3.cloned.1.call-update) | async-done | bytes 4194320 | tf_op jit(solution)/shard_map/all_gather | solution.py:201
  190.3 3.7 %convolution_convert_fusion = bf16[128,2048]{1,0:T(8,128)(2,1)} fusion(bf16[1024,128]{1,0:T(8,128)(2,1)S(1)} %bitcast.189, bf16[1024,2048]{1,0:T(8,128)(2,1)} %all-gather.3.cloned.1.call-done), kind=kOutput, calls=%fused_computation.13 | convolution fusion | flops 537133056 | bytes 4980736 | tf_op jit(solution)/shard_map/cr,cm->rm/dot_general | solution.py:203
  194.0 16.0 %all-to-all-done.3 = bf16[32,1,16,2048]{3,2,1,0:T(8,128)(2,1)S(1)} async-done(((bf16[32,1,16,2048]{3,2,1,0:T(8,128)(2,1)}), bf16[32,1,16,2048]{3,2,1,0:T(8,128)(2,1)S(1)}, u32[]{:S(2)}, u32[]{:S(2)}) %all-to-all-start.3) | async-done | bytes 2097184 | tf_op jit(solution)/shard_map/all_to_all | solution.py:248
  212.8 3.9 %multiply_reduce_fusion = bf16[128,2048]{1,0:T(8,128)(2,1)} fusion(f32[128,2,2048]{2,1,0:T(2,128)S(1)} %reshape.181, f32[128,2]{1,0:T(8,128)S(1)} %copy.108), kind=kLoop, calls=%fused_computation.23 | loop fusion | flops 786432 | bytes 2622464 | tf_op jit(solution)/shard_map/reduce_sum | solution.py:251
  (92 shorter events, 20.4 us)
Async XLA Ops:
  7.2 145.4 %all-gather.5.cloned.1.call-start = ((), (), s32[]{:S(2)}) async-start(), calls=%async_computation.5 | async-start | bytes 15728640 | tf_op jit(solution)/shard_map/all_gather | solution.py:209
  11.7 0.9 copy-start.1
  11.7 1.5 copy-start.2
  17.2 9.8 %copy-start.3 = (bf16[512,256]{1,0:T(8,128)(2,1)S(1)}, bf16[512,256]{1,0:T(8,128)(2,1)}, u32[]{:S(2)}) copy-start(bf16[512,256]{1,0:T(8,128)(2,1)} %param.12) | copy-start | bytes 786436
  17.2 19.0 %copy-start.5 = (s32[128,2]{0,1:T(2,128)S(1)}, s32[128,2]{0,1:T(2,128)}, u32[]{:S(2)}) copy-start(s32[128,2]{0,1:T(2,128)} %param.19) | copy-start | bytes 3076
  17.2 61.5 %all-to-all-start = ((bf16[32,512,128]{2,1,0:T(8,128)(2,1)}), bf16[32,512,128]{2,1,0:T(8,128)(2,1)}, u32[]{:S(2)}, u32[]{:S(2)}) async-start(bf16[32,512,128]{2,1,0:T(8,128)(2,1)} %bitcast.186), calls=%async_computation | async-start | bytes 8388608 | tf_op jit(solution)/shard_map/all_to_all | solution.py:179
  27.0 12.6 %copy-start = (bf16[128,2048]{1,0:T(8,128)(2,1)S(1)}, bf16[128,2048]{1,0:T(8,128)(2,1)}, u32[]{:S(2)}) copy-start(bf16[128,2048]{1,0:T(8,128)(2,1)} %param.17) | copy-start | bytes 1572868
  27.0 12.7 %copy-start.4 = (f32[2048]{0:T(1024)S(1)}, f32[2048]{0:T(1024)}, u32[]{:S(2)}) copy-start(f32[2048]{0:T(1024)} %param.18) | copy-start | bytes 24580
  27.4 48.0 %collective-permute-start.2 = (bf16[64,512]{1,0:T(8,128)(2,1)S(1)}, bf16[64,512]{1,0:T(8,128)(2,1)S(1)}, u32[]{:S(2)}, u32[]{:S(2)}) collective-permute-start(bf16[64,512]{1,0:T(8,128)(2,1)S(1)} %get-tuple-element.7), channel_id=1, source_target_pairs={{0,16},{4,20},{8,48},{12,52},{16,80},{20,84},{24,112},{28,116},{32... | collective-permute-start | bytes 196616 | tf_op jit(solution)/shard_map/ppermute | solution.py:185
  30.3 46.0 %collective-permute-start.3 = (bf16[64,512]{1,0:T(8,128)(2,1)S(1)}, bf16[64,512]{1,0:T(8,128)(2,1)S(1)}, u32[]{:S(2)}, u32[]{:S(2)}) collective-permute-start(bf16[64,512]{1,0:T(8,128)(2,1)S(1)} %get-tuple-element.9), channel_id=1, source_target_pairs={{0,24},{4,28},{8,56},{12,60},{16,88},{20,92},{24,120},{28,124},{32... | collective-permute-start | bytes 196616 | tf_op jit(solution)/shard_map/ppermute | solution.py:185
  32.8 43.5 %collective-permute-start = (bf16[64,512]{1,0:T(8,128)(2,1)S(1)}, bf16[64,512]{1,0:T(8,128)(2,1)S(1)}, u32[]{:S(2)}, u32[]{:S(2)}) collective-permute-start(bf16[64,512]{1,0:T(8,128)(2,1)S(1)} %get-tuple-element.6), channel_id=1, source_target_pairs={{0,0},{4,4},{8,32},{12,36},{16,64},{20,68},{24,96},{28,100},{32,10... | collective-permute-start | bytes 196616 | tf_op jit(solution)/shard_map/ppermute | solution.py:185
  33.4 44.5 %collective-permute-start.1 = (bf16[64,512]{1,0:T(8,128)(2,1)S(1)}, bf16[64,512]{1,0:T(8,128)(2,1)S(1)}, u32[]{:S(2)}, u32[]{:S(2)}) collective-permute-start(bf16[64,512]{1,0:T(8,128)(2,1)S(1)} %get-tuple-element.8), channel_id=1, source_target_pairs={{0,8},{4,12},{8,40},{12,44},{16,72},{20,76},{24,104},{28,108},{32,... | collective-permute-start | bytes 196616 | tf_op jit(solution)/shard_map/ppermute | solution.py:185
  78.7 69.8 %all-to-all-start.2 = ((bf16[32,1,16,2048]{3,2,1,0:T(8,128)(2,1)}), bf16[32,1,16,2048]{3,2,1,0:T(8,128)(2,1)S(1)}, u32[]{:S(2)}, u32[]{:S(2)}) async-start(bf16[32,1,16,2048]{3,2,1,0:T(8,128)(2,1)} %bitcast.52), calls=%async_computation.2 | async-start | bytes 4194304 | tf_op jit(solution)/shard_map/all_to_all | solution.py:245
  87.7 102.6 %all-gather.3.cloned.1.call-start = ((), (), s32[]{:S(2)}) async-start(), calls=%async_computation.4 | async-start | bytes 5242880 | tf_op jit(solution)/shard_map/all_gather | solution.py:201
  133.2 8.4 %collective-permute-start.4 = (bf16[64,512]{1,0:T(8,128)(2,1)S(1)}, bf16[64,512]{1,0:T(8,128)(2,1)S(1)}, u32[]{:S(2)}, u32[]{:S(2)}) collective-permute-start(bf16[64,512]{1,0:T(8,128)(2,1)S(1)} %get-tuple-element.5), channel_id=1, source_target_pairs={{0,0},{4,4},{32,8},{36,12},{64,16},{68,20},{96,24},{100,28},{108,3... | collective-permute-start | bytes 196616 | tf_op jit(solution)/shard_map/ppermute | solution.py:196
  133.9 9.3 %collective-permute-start.5 = (bf16[64,512]{1,0:T(8,128)(2,1)S(1)}, bf16[64,512]{1,0:T(8,128)(2,1)S(1)}, u32[]{:S(2)}, u32[]{:S(2)}) collective-permute-start(bf16[64,512]{1,0:T(8,128)(2,1)S(1)} %get-tuple-element.4), channel_id=1, source_target_pairs={{8,0},{12,4},{40,8},{44,12},{72,16},{76,20},{104,24},{108,28},{116... | collective-permute-start | bytes 196616 | tf_op jit(solution)/shard_map/ppermute | solution.py:196
  140.5 5.4 %collective-permute-start.6 = (bf16[64,512]{1,0:T(8,128)(2,1)S(1)}, bf16[64,512]{1,0:T(8,128)(2,1)S(1)}, u32[]{:S(2)}, u32[]{:S(2)}) collective-permute-start(bf16[64,512]{1,0:T(8,128)(2,1)S(1)} %get-tuple-element.3), channel_id=1, source_target_pairs={{16,0},{20,4},{48,8},{52,12},{80,16},{84,20},{112,24},{116,28},{12... | collective-permute-start | bytes 196616 | tf_op jit(solution)/shard_map/ppermute | solution.py:196
  141.3 6.3 %collective-permute-start.7 = (bf16[64,512]{1,0:T(8,128)(2,1)S(1)}, bf16[64,512]{1,0:T(8,128)(2,1)S(1)}, u32[]{:S(2)}, u32[]{:S(2)}) collective-permute-start(bf16[64,512]{1,0:T(8,128)(2,1)S(1)} %get-tuple-element.2), channel_id=1, source_target_pairs={{24,0},{28,4},{56,8},{60,12},{88,16},{92,20},{120,24},{124,28},{10... | collective-permute-start | bytes 196616 | tf_op jit(solution)/shard_map/ppermute | solution.py:196
  148.5 24.6 %all-to-all-start.1 = ((bf16[4,256,128]{2,1,0:T(8,128)(2,1)}), bf16[4,256,128]{2,1,0:T(8,128)(2,1)S(1)}, u32[]{:S(2)}, u32[]{:S(2)}) async-start(bf16[4,256,128]{2,1,0:T(8,128)(2,1)} %copy.98), calls=%async_computation.1 | async-start | bytes 524288 | tf_op jit(solution)/shard_map/all_to_all | solution.py:200
  173.1 8.5 %copy-start.6 = (f32[128,2]{0,1:T(2,128)S(1)}, f32[128,2]{0,1:T(2,128)}, u32[]{:S(2)}) copy-start(f32[128,2]{0,1:T(2,128)} %param.20) | copy-start | bytes 3076
  173.1 37.0 %all-to-all-start.3 = ((bf16[32,1,16,2048]{3,2,1,0:T(8,128)(2,1)}), bf16[32,1,16,2048]{3,2,1,0:T(8,128)(2,1)S(1)}, u32[]{:S(2)}, u32[]{:S(2)}) async-start(bf16[32,1,16,2048]{3,2,1,0:T(8,128)(2,1)} %copy.107), calls=%async_computation.3 | async-start | bytes 4194304 | tf_op jit(solution)/shard_map/all_to_all | solution.py:248
Sparse Core Ops, SparseCore 0:
  11.9 124.1 all-gather.4
  137.7 52.5 all-gather.2

commit v2 on v1

--- a/solution.py
+++ b/solution.py
@@ -6,6 +6,7 @@
 from jax.experimental import pallas as pl
 from jax.experimental.pallas import tpu as pltpu
 from jax.sharding import PartitionSpec as P
+
 
 HEAD_DIM = 64
 GROUPS = 4
@@ -16,10 +17,11 @@
 RUN = HALF // RUNS
 LOG2E = math.log2(math.e)
 U_CAP = 48.0
+MESH = pl.DeviceIdType.MESH
 norm_eps = 1e-06
 
 
-def attend_kernel(tiles_ref, qt_ref, kv_ref, bias_ref, out_ref, kk_ref, rhs_ref, z_hi, z_lo, w_hi, w_lo, acc_ref, carry_ref):
+def attend_kernel(tiles_ref, qt_ref, kv_ref, rows_ref, out_ref, kk_ref, bias_ref, rhs_ref, z_hi, z_lo, w_hi, w_lo, acc_ref, carry_ref):
     lanes = qt_ref.shape[2]
     low_lane = lax.broadcasted_iota(jnp.int32, (HALF, 128), 1) < HEAD_DIM
     sub = lax.broadcasted_iota(jnp.int32, (RUNS, 128), 0)
@@ -30,6 +32,14 @@
         turned = pltpu.roll(pair, HEAD_DIM, axis=1)
         kk_ref[b, 0] = jnp.where(low_lane, pair, turned).astype(jnp.bfloat16)
         kk_ref[b, 1] = jnp.where(low_lane, turned, pair).astype(jnp.bfloat16)
+        for half in range(2):
+            value = rows_ref[b, half : half + 1, :] * LOG2E
+            parts = jnp.zeros((128, HALF), jnp.float32)
+            for n in range(3):
+                part = value.astype(jnp.bfloat16).astype(jnp.float32)
+                parts = jnp.where(row[:, 0:HALF] == n, part, parts)
+                value = value - part
+            bias_ref[b, half] = parts.T.astype(jnp.bfloat16)
         return carried
 
     lax.fori_loop(0, kv_ref.shape[0], build, 0)
@@ -121,6 +131,7 @@
         out_specs=whole,
         scratch_shapes=[
             pltpu.VMEM((blocks, 2, HALF, 128), jnp.bfloat16),
+            pltpu.VMEM((blocks, 2, HALF, 128), jnp.bfloat16),
             pltpu.VMEM((HALF, lanes), jnp.bfloat16),
             pltpu.VMEM((HALF, lanes), jnp.float32),
             pltpu.VMEM((HALF, lanes), jnp.float32),
@@ -129,7 +140,7 @@
             pltpu.VMEM((width, lanes), jnp.float32),
             pltpu.VMEM((RUNS, lanes), jnp.float32),
         ],
-        cost_estimate=pl.CostEstimate(flops=40_000_000_000, bytes_accessed=12 << 20, transcendentals=0),
+        cost_estimate=pl.CostEstimate(flops=20_000_000_000, bytes_accessed=12 << 20, transcendentals=0),
         name="stick_attend",
     )(tiles, qt, kv, bias)
 
@@ -139,15 +150,123 @@
     return rows.reshape(2, RUNS, RUN, n).swapaxes(1, 2).reshape(BLOCK, n)
 
 
-def bias_lanes(bias):
-    left = bias * LOG2E
-    lane = lax.broadcasted_iota(jnp.int32, bias.shape[:3] + (128,), 3)
-    out = jnp.zeros(lane.shape, jnp.float32)
-    for n in range(3):
-        part = lax.reduce_precision(left, 8, 7)
-        out = jnp.where(lane == n, part, out)
-        left = left - part
-    return out.astype(jnp.bfloat16)
+def turn_of(block):
+    slot, at = block // 8, block % 8
+    return jnp.where(slot % 2 == 0, at, 7 - at)
+
+
+def block_of(slot, turn):
+    return slot * 8 + jnp.where(slot % 2 == 0, turn, 7 - turn)
+
+
+def exchange_kernel(kv_ref, q_ref, kv_out, q_out, got, q_got, s_col, s_up, s_down, s_pair, s_q, s_own):
+    me = lax.axis_index("ep")
+    z, y, c = me // 8, me // 2 % 4, me % 2
+    turn = 2 * z + c
+    my_slot, my_turn = z, turn_of(me)
+
+    def at(zz, yy, cc):
+        return (zz + 4) % 4 * 8 + (yy + 4) % 4 * 2 + cc
+
+    def dest(index):
+        return {"ep": index}
+
+    def q_dest(h):
+        return my_turn // 2 * 8 + 2 * h + my_turn % 2
+
+    barrier = pltpu.get_barrier_semaphore()
+    near = [at(z, y + d, c) for d in (1, 2, 3)] + [at(z + 1, y, c), at(z - 1, y, c), at(z, y, 1 - c)]
+    for index in near:
+        pl.semaphore_signal(barrier, inc=1, device_id=dest(index), device_id_type=MESH)
+    alone = (my_turn == turn).astype(jnp.int32)
+    for h in range(4):
+        @pl.when(q_dest(h) != me)
+        def _():
+            pl.semaphore_signal(barrier, inc=1, device_id=dest(q_dest(h)), device_id_type=MESH)
+
+        @pl.when(block_of(h, turn) != me)
+        def _():
+            pl.semaphore_signal(barrier, inc=1, device_id=dest(block_of(h, turn)), device_id_type=MESH)
+    pl.semaphore_wait(barrier, len(near) + 8 - 2 * alone)
+
+    def send(src, index, dst, send_sem, recv_sem):
+        copy = pltpu.make_async_remote_copy(
+            src_ref=src, dst_ref=dst, send_sem=send_sem, recv_sem=recv_sem,
+            device_id=dest(index), device_id_type=MESH,
+        )
+        copy.start()
+        return copy
+
+    def piece(index):
+        return kv_out.at[index]
+
+    def arrived(index):
+        pltpu.make_async_copy(piece(index), piece(index), got.at[index]).wait()
+
+    sent = []
+    for d in (1, 2, 3):
+        sent.append(send(kv_ref.at[(y + d) % 4], at(z, y + d, c), piece(me), s_col.at[d - 1], got.at[me]))
+    for h in range(4):
+        @pl.when(q_dest(h) != me)
+        def _():
+            send(q_ref.at[h], q_dest(h), q_out.at[my_slot], s_q.at[h], q_got.at[my_slot])
+
+        @pl.when(q_dest(h) == me)
+        def _():
+            pltpu.make_async_copy(q_ref.at[h], q_out.at[my_slot], q_got.at[my_slot]).start()
+    own = pltpu.make_async_copy(kv_ref.at[y], piece(me), s_own)
+    own.start()
+    for d in range(4):
+        index = at(z, y - d, c)
+        if d > 0:
+            arrived(index)
+        src = kv_ref.at[y] if d == 0 else piece(index)
+        sent.append(send(src, at(z + 1, y, c), piece(index), s_up.at[d], got.at[index]))
+        sent.append(send(src, at(z - 1, y, c), piece(index), s_down.at[d], got.at[index]))
+        sent.append(send(src, at(z, y, 1 - c), piece(index), s_pair.at[d], got.at[index]))
+    for d in range(4):
+        for n, dz in enumerate((1, -1)):
+            index = at(z - dz, y - d, c)
+            arrived(index)
+            if d < 2 and dz == 1:
+                sent.append(send(piece(index), at(z + 1, y, c), piece(index), s_up.at[4 + d], got.at[index]))
+            if d >= 2 and dz == -1:
+                sent.append(send(piece(index), at(z - 1, y, c), piece(index), s_down.at[2 + d], got.at[index]))
+            sent.append(send(piece(index), at(z, y, 1 - c), piece(index), s_pair.at[4 + 2 * d + n], got.at[index]))
+    for d in (0, 2, 1, 3):
+        index = at(z + 2, y - d, c)
+        arrived(index)
+        sent.append(send(piece(index), at(z, y, 1 - c), piece(index), s_pair.at[12 + d], got.at[index]))
+    for k in range(4):
+        pltpu.make_async_copy(q_out.at[k], q_out.at[k], q_got.at[k]).wait()
+    for zz in range(4):
+        for yy in range(4):
+            arrived(at(zz, yy, 1 - c))
+    own.wait()
+    for copy in sent:
+        copy.wait_send()
+    for h in range(4):
+        @pl.when(q_dest(h) != me)
+        def _():
+            pltpu.make_async_copy(q_ref.at[h], q_ref.at[h], s_q.at[h]).wait()
+
+
+def exchange(kv, q):
+    whole = pl.BlockSpec(memory_space=pltpu.VMEM)
+    dma = pltpu.SemaphoreType.DMA
+    return pl.pallas_call(
+        exchange_kernel,
+        out_shape=(
+            jax.ShapeDtypeStruct((32,) + kv.shape[1:], kv.dtype),
+            jax.ShapeDtypeStruct(q.shape, q.dtype),
+        ),
+        in_specs=[whole, whole],
+        out_specs=(whole, whole),
+        scratch_shapes=[dma((32,)), dma((4,)), dma((3,)), dma((6,)), dma((6,)), dma((16,)), dma((4,)), dma],
+        compiler_params=pltpu.CompilerParams(collective_id=1, has_side_effects=True),
+        cost_estimate=pl.CostEstimate(flops=20_000_000_000, bytes_accessed=8 << 20, transcendentals=0),
+        name="exchange",
+    )(kv, q)
 
 
 def slot_and_turn(block):
@@ -155,73 +274,62 @@
     return slot, at if slot % 2 == 0 else 7 - at
 
 
-def routes(turn):
+def homeward(step):
     pairs = []
     for block in range(32):
         slot, j = slot_and_turn(block)
-        pairs.append((block, j // 2 * 8 + (slot + turn) % 4 * 2 + j % 2))
+        head = (slot + step) % 4
+        pairs.append((j // 2 * 8 + head * 2 + j % 2, block))
     return pairs
 
 
 def mixer(query_rows, key_rows, value_rows, key_bias, out_weight):
     ep_index = lax.axis_index("ep")
-    head = ep_index // 2 % 4
-    turn = ep_index // 8 * 2 + ep_index % 2
-    my_slot = ep_index // 8
+    head = (ep_index >> 1) & 3
+    turn = (ep_index >> 3) * 2 + (ep_index & 1)
+    my_slot = ep_index >> 3
 
     q_heads = query_rows.T.reshape(4, HEAD_DIM, BLOCK)
     keys = key_order(key_rows).reshape(2, HALF, 4, HEAD_DIM)
     k_heads = keys.transpose(2, 1, 0, 3).reshape(4, HALF, 128)
     values = key_order(value_rows).T.reshape(4, HEAD_DIM, 4, 128)
     v_heads = values.transpose(0, 2, 1, 3).reshape(4, HALF, 128)
-    kv_heads = jnp.concatenate([k_heads, v_heads], axis=1)
-    kv_out = jnp.broadcast_to(kv_heads[None, :, None], (4, 4, 2, BLOCK, 128)).reshape(32, BLOCK, 128)
-    kv = lax.all_to_all(kv_out, "ep", split_axis=0, concat_axis=0, tiled=True)
-
-    q_twice = jnp.concatenate([q_heads, q_heads], axis=0)
-    q_got, tiles = [], []
+    kv, qt = exchange(jnp.concatenate([k_heads, v_heads], axis=1), q_heads)
+
+    column = lax.dynamic_slice_in_dim(key_bias, head, 1, 1)
+    bias = column.reshape(32, 2, RUNS, RUN).swapaxes(2, 3).reshape(32, 2, HALF)
+    done_a = attend(jnp.stack([turn, 31 - turn]).astype(jnp.int32), jnp.stack([qt[0], qt[3]]), kv, bias)
+    done_b = attend(jnp.stack([15 - turn, 16 + turn]).astype(jnp.int32), qt[1:3], kv, bias)
+    done = jnp.stack([done_a[0], done_b[0], done_b[1], done_a[1]])
+
+    twice = jnp.concatenate([done, done], axis=0)
+    back = []
     for r in range(4):
-        mine = lax.dynamic_index_in_dim(q_twice, my_slot + r, 0, keepdims=False)
-        q_got.append(lax.ppermute(mine, "ep", routes(r)))
-        slot = (head - r + 4) % 4
-        tiles.append(slot * 8 + jnp.where(slot % 2 == 0, turn, 7 - turn))
-    qt = jnp.stack(q_got)
-    tiles = jnp.stack(tiles).astype(jnp.int32)
-
-    column = lax.dynamic_slice_in_dim(key_bias, head, 1, 1)
-    bias = bias_lanes(column.reshape(32, 2, RUNS, RUN, 1).swapaxes(2, 3).reshape(32, 2, HALF, 1))
-
-    done = attend(tiles, qt, kv, bias)
-
-    back = [lax.ppermute(done[r], "ep", [(b, a) for a, b in routes(r)]) for r in range(4)]
-    twice = jnp.stack(back + back)
-    attended = lax.dynamic_slice_in_dim(twice, 4 - my_slot, 4, 0)
-    pieces = attended.reshape(4 * HEAD_DIM, 4, 128).swapaxes(0, 1)
-    columns = lax.all_to_all(pieces, "tp", split_axis=0, concat_axis=0, tiled=True)
-    weight = lax.all_gather(out_weight, "tp", axis=0, tiled=True)
-    columns = columns.reshape(weight.shape[0], 128)
-    return jnp.einsum("cr,cm->rm", columns, weight, preferred_element_type=jnp.float32).astype(jnp.bfloat16)
-
-
-def gather_turned(arrays, axis, dims):
-    turned = [jnp.moveaxis(a, dim, 0) for a, dim in zip(arrays, dims)]
-    both = jnp.concatenate([t.reshape(len(t), -1) for t in turned], axis=1)
-    filled, at, done = (lax.all_gather(both, axis, axis=0, tiled=True), 0, [])
-    for t, dim in zip(turned, dims):
-        slab = filled[:, at : at + t[0].size].reshape(-1, *t.shape[1:])
-        done.append(jnp.moveaxis(slab, 0, dim))
-        at += t[0].size
-    return tuple(done)
-
-
-def expand(arrived, gate_weights, up_weights):
-    gate_in = jnp.einsum("necm,emf->necf", arrived, gate_weights, preferred_element_type=jnp.float32)
-    up_in = jnp.einsum("necm,emf->necf", arrived, up_weights, preferred_element_type=jnp.float32)
-    return (jax.nn.silu(gate_in) * up_in).astype(jnp.bfloat16)
-
-
-def contract(hidden, down_weights):
-    return jnp.einsum("necf,efm->necm", hidden, down_weights, preferred_element_type=jnp.float32)
+        mine = lax.dynamic_index_in_dim(twice, (head - r) & 3, 0, keepdims=False)
+        back.append(lax.ppermute(mine, "ep", homeward(r)))
+    rows = [lax.dynamic_slice_in_dim(out_weight, ((my_slot + r) & 3) * HEAD_DIM, HEAD_DIM, 0) for r in range(4)]
+    attended = jnp.concatenate(back, axis=0)
+    part = jnp.einsum("cr,cm->rm", attended, jnp.concatenate(rows, axis=0), preferred_element_type=jnp.float32)
+    pieces = part.astype(jnp.bfloat16).reshape(4, 128, part.shape[1])
+    arrived = lax.all_to_all(pieces, "tp", split_axis=0, concat_axis=0, tiled=True)
+    return arrived.astype(jnp.float32).sum(axis=0).astype(jnp.bfloat16)
+
+
+RIGHT = [(i, (i + 1) % 4) for i in range(4)]
+LEFT = [(i, (i + 3) % 4) for i in range(4)]
+
+
+def neighbours(shard):
+    return lax.ppermute(shard, "tp", RIGHT), lax.ppermute(shard, "tp", LEFT)
+
+
+def opposite(from_left, from_right):
+    half = from_left.shape[0] // 2
+    return lax.ppermute(from_left[:half], "tp", RIGHT), lax.ppermute(from_right[half:], "tp", LEFT)
+
+
+def dot(a, b):
+    return jnp.dot(a, b, preferred_element_type=jnp.float32)
 
 
 def experts(moe_input, moe_gain, expert_pick, route_weight, w_gate, w_up, w_down):
@@ -243,8 +351,20 @@
     padded = jnp.concatenate([normed, jnp.zeros((1, normed.shape[1]), jnp.bfloat16)], axis=0)
     outgoing = padded[table].reshape(ep_count, local_experts, capacity, normed.shape[1])
     arrived = lax.all_to_all(outgoing, "ep", split_axis=0, concat_axis=0, tiled=True)
-    gate_all, up_all, down_all = gather_turned((w_gate, w_up, w_down), "tp", (2, 2, 1))
-    served = contract(expand(arrived, gate_all, up_all), down_all).astype(jnp.bfloat16)
+    rows = arrived.reshape(expert_total * capacity, normed.shape[1])
+    both = jnp.concatenate([w_gate[0], w_up[0]], axis=1)
+    both_left, both_right = neighbours(both)
+    down_left, down_right = neighbours(w_down[0])
+    both_a, both_b = opposite(both_left, both_right)
+    down_a, down_b = opposite(down_left, down_right)
+    half = both.shape[0] // 2
+    ins = [dot(rows, part) for part in (both, both_left, both_right)]
+    ins.append(dot(rows[:, :half], both_a) + dot(rows[:, half:], both_b))
+    width = w_gate.shape[2]
+    hidden = [(jax.nn.silu(v[:, :width]) * v[:, width:]).astype(jnp.bfloat16) for v in ins]
+    downs = jnp.concatenate([w_down[0], down_left, down_right, down_a, down_b], axis=0)
+    served = dot(jnp.concatenate(hidden, axis=1), downs).astype(jnp.bfloat16)
+    served = served.reshape(ep_count, local_experts, capacity, normed.shape[1])
     returned = lax.all_to_all(served, "ep", split_axis=0, concat_axis=0, tiled=True)
     flat = returned.reshape(expert_total * capacity, returned.shape[3])
     chosen = flat[slots].reshape(token_count, TOPK, flat.shape[1]).astype(jnp.float32)

time: 225 us -> 293 us (1.30)
  Pallas kernels: 44.5 us -> 89.3 us
  waiting for transfers between devices: 54.4 us -> 95.3 us
  between operations: 14.6 us -> 1.09 us
  local copies, waits for them, and re-layouts: 21.9 us -> 32.5 us
  starting transfers between devices: 48.5 us -> 39.9 us
  other arithmetic: 19.5 us -> 13.9 us
    ppermute x8 -> x12, waiting for transfers between devices: 29.7 us -> 69.8 us  [the longest x2 30.7 us: opposite(): lax.ppermute(from_right[half:], 'tp', LEFT)]
    pallas_call x0 -> x1, Pallas kernels: none -> 37 us  [exchange(): pl.pallas_call(exchange_kernel, out_shape=(jax.ShapeDtypeStruct((32,) + k...]
    all_to_all x1 -> x0, starting transfers between devices: 9.78 us -> none  [mixer(): kv = lax.all_to_all(kv_out, 'ep', split_axis=0, concat_axis=0, tiled=True)]
    all_to_all x1, waiting for transfers between devices: 16 us -> 25.5 us  [experts(): lax.all_to_all(served, 'ep', split_axis=0, concat_axis=0, tiled=True)]
    all_gather x2 -> x0, waiting for transfers between devices: 8.64 us -> none  [the longest x1 8.64 us: mixer(): weight = lax.all_gather(out_weight, 'tp', axis=0, tiled=True)]
    unnamed x25 -> x35, local copies, waits for them, and re-layouts: 2.84 us -> 11 us
    convert_element_type x1 -> x4, other arithmetic: 8.62 us -> 0.63 us  [experts(): (jax.nn.silu(v[:, :width]) * v[:, width:]).astype(jnp.bfloat16)]
    pallas_call x1 -> x2, Pallas kernels: 44.5 us -> 52.2 us  [attend(): pl.pallas_call(attend_kernel, out_shape=jax.ShapeDtypeStruct((n_tiles, wi...]
  transfers between devices with their start and end apart: 14 -> 15, of which waited for: 8 -> 7; matrix products, arithmetic and copies ran while one was open for 22% -> 19% of each run, Pallas kernels for 20% -> 31%
where the time goes in v2:
time: 293 us; the launch traced here: 292 us
  waiting for transfers between devices  95.3 us (33%)
  Pallas kernels  89.3 us (30%)
  starting transfers between devices  39.9 us (14%)
  local copies, waits for them, and re-layouts  32.5 us (11%)
  matrix products  19.6 us (7%)
  other arithmetic  13.9 us (5%)
    pallas_call x2, Pallas kernels, attend(): pl.pallas_call(attend_kernel, out_shape=jax.ShapeDtypeStruct((n_tiles, wi...  52.2 us
    pallas_call x1, Pallas kernels, exchange(): pl.pallas_call(exchange_kernel, out_shape=(jax.ShapeDtypeStruct((32,) + k...  37 us
    ppermute x2, waiting for transfers between devices, opposite(): lax.ppermute(from_right[half:], 'tp', LEFT)  30.7 us
    all_to_all x1, waiting for transfers between devices, experts(): lax.all_to_all(served, 'ep', split_axis=0, concat_axis=0, tiled=True)  25.5 us
    ppermute x2, waiting for transfers between devices, opposite(): lax.ppermute(from_left[:half], 'tp', RIGHT)  20.4 us
    ppermute x4, waiting for transfers between devices, mixer(): back.append(lax.ppermute(mine, 'ep', homeward(r)))  18.7 us
    dot_general x6, matrix products, dot(): return jnp.dot(a, b, preferred_element_type=jnp.float32)  16.7 us
    ppermute x4, starting transfers between devices, mixer(): back.append(lax.ppermute(mine, 'ep', homeward(r)))  11.4 us
  transfers between devices with their start and end apart: 15, of which 7 were waited for; matrix products, arithmetic and copies ran while one was open for 19% of the time, Pallas kernels for 31%

profile of v2, /device:TPU:1, one launch (start us, length us, event | category | flops | bytes accessed | tf_op | source)
XLA Modules:
  0.0 291.6 jit_solution(16213197336461017816)
XLA Ops:
  8.1 37.0 %exchange.1 = (bf16[32,512,128]{2,1,0:T(8,128)(2,1)}, bf16[4,64,512]{2,1,0:T(8,128)(2,1)}) custom-call(bf16[4,512,128]{2,1,0:T(8,128)(2,1)} %pad_maximum_fusion.1.kv_ref, bf16[4,64,512]{2,1,0:T(8,128)(2,1)} %bitcast.99), custom_call_target="tpu_custom_call" | custom-call | flops 20000000000 | bytes 8388608 | tf_op jit(solution)/shard_map/exchange/pallas_call | solution.py:257
  50.1 26.1 %stick_attend.2 = bf16[2,64,512]{2,1,0:T(8,128)(2,1)} custom-call(s32[2]{0:T(128)} %get-tuple-element.16.tiles_ref, bf16[2,64,512]{2,1,0:T(8,128)(2,1)} %pad_maximum_fusion.2.qt_ref, bf16[32,512,128]{2,1,0:T(8,128)(2,1)} %get-tuple-element.5.kv_ref, f32[32,2,256]{2,1,0:T(2,128)} %copy.53.rows_ref), custom_call_target="tpu_custom_call" | custom-call | flops 20000000000 | bytes 12582912 | tf_op jit(solution)/shard_map/stick_attend/pallas_call | solution.py:127
  77.1 26.1 %stick_attend.3 = bf16[2,64,512]{2,1,0:T(8,128)(2,1)} custom-call(s32[2]{0:T(128)} %get-tuple-element.17.tiles_ref, bf16[2,64,512]{2,1,0:T(8,128)(2,1)} %slice.70.qt_ref, bf16[32,512,128]{2,1,0:T(8,128)(2,1)} %get-tuple-element.5.kv_ref, f32[32,2,256]{2,1,0:T(2,128)} %copy.53.rows_ref), custom_call_target="tpu_custom_call" | custom-call | flops 20000000000 | bytes 12582912 | tf_op jit(solution)/shard_map/stick_attend/pallas_call | solution.py:127
  105.8 2.1 collective-permute-start
  111.5 3.3 %gather_fusion = bf16[512,2048]{1,0:T(8,128)(2,1)} fusion(bf16[129,2048]{1,0:T(8,128)(2,1)S(1)} %concatenate.30, s32[1024]{0:T(1024)S(1)} %pad_clamp_fusion.1), kind=kCustom, calls=%fused_computation | custom fusion | bytes 4196352 | tf_op jit(solution)/shard_map/gather | solution.py:352
  114.8 6.8 %all-to-all-start.1 = ((bf16[32,1,16,2048]{3,2,1,0:T(8,128)(2,1)}), bf16[32,1,16,2048]{3,2,1,0:T(8,128)(2,1)S(1)}, u32[]{:S(2)}, u32[]{:S(2)}) async-start(bf16[32,1,16,2048]{3,2,1,0:T(8,128)(2,1)} %bitcast.27), calls=%async_computation.1 | async-start | bytes 4194304 | tf_op jit(solution)/shard_map/all_to_all | solution.py:353
  121.6 3.1 %pad_maximum_fusion = bf16[2048,512]{1,0:T(8,128)(2,1)} fusion(bf16[2048,256]{1,0:T(8,128)(2,1)} %bitcast.92, bf16[2048,256]{1,0:T(8,128)(2,1)} %bitcast.94), kind=kLoop, calls=%fused_computation.5 | loop fusion | flops 4194304 | bytes 4194304 | tf_op jit(solution)/shard_map/concatenate | solution.py:355
  126.2 5.6 %collective-permute-start.1 = (bf16[64,512]{1,0:T(8,128)(2,1)}, bf16[64,512]{1,0:T(8,128)(2,1)}, u32[]{:S(2)}, u32[]{:S(2)}) collective-permute-start(bf16[64,512]{1,0:T(8,128)(2,1)} %get-tuple-element.13), channel_id=1, source_target_pairs={{8,0},{12,4},{40,8},{44,12},{72,16},{76,20},{104,24},{108,28},{116... | collective-permute-start | bytes 196616 | tf_op jit(solution)/shard_map/ppermute | solution.py:309
  132.8 15.2 %collective-permute-done.1 = bf16[64,512]{1,0:T(8,128)(2,1)} collective-permute-done((bf16[64,512]{1,0:T(8,128)(2,1)}, bf16[64,512]{1,0:T(8,128)(2,1)}, u32[]{:S(2)}, u32[]{:S(2)}) %collective-permute-start.1) | collective-permute-done | bytes 65568 | tf_op jit(solution)/shard_map/ppermute | solution.py:309
  148.1 3.7 %collective-permute-start.2 = (bf16[64,512]{1,0:T(8,128)(2,1)S(1)}, bf16[64,512]{1,0:T(8,128)(2,1)S(1)}, u32[]{:S(2)}, u32[]{:S(2)}) collective-permute-start(bf16[64,512]{1,0:T(8,128)(2,1)S(1)} %get-tuple-element.12), channel_id=1, source_target_pairs={{16,0},{20,4},{48,8},{52,12},{80,16},{84,20},{112,24},{116,28},{12... | collective-permute-start | bytes 196616 | tf_op jit(solution)/shard_map/ppermute | solution.py:309
  156.5 2.9 %convolution_convert_fusion.1 = bf16[512,2048]{1,0:T(8,128)(2,1)} fusion(bf16[64,2048]{1,0:T(8,128)(2,1)S(1)} %get-tuple-element.8, bf16[64,2048]{1,0:T(8,128)(2,1)S(1)} %get-tuple-element.9, bf16[64,2048]{1,0:T(8,128)(2,1)S(1)} %get-tuple-element.7, bf16[64,2048]{1,0:T(8,128)(2,1)S(1)} %get-tuple-element.6, bf16[64,512]{1,0:T(8,128)(2,1)S(1)} %collective-permute-done.3, ...), kind=kOutput, calls=%fused_computation.4 | convolution fusion | flops 543162368 | bytes 3407872 | tf_op jit(solution)/shard_map/cr,cm->rm/dot_general | solution.py:312
  163.0 2.3 constant_dynamic-update-slice_fusion.4
  165.3 20.0 %collective-permute-done.10 = bf16[128,2048]{1,0:T(8,128)(2,1)S(1)} collective-permute-done((bf16[128,2048]{1,0:T(8,128)(2,1)S(1)}, bf16[128,2048]{1,0:T(8,128)(2,1)S(1)}, u32[]{:S(2)}, u32[]{:S(2)}) %collective-permute-start.10) | collective-permute-done | bytes 524320 | tf_op jit(solution)/shard_map/ppermute | solution.py:328
  188.3 3.6 %all-to-all-start = ((bf16[4,128,2048]{2,1,0:T(8,128)(2,1)}), bf16[4,128,2048]{2,1,0:T(8,128)(2,1)S(1)}, u32[]{:S(2)}, u32[]{:S(2)}) async-start(bf16[4,128,2048]{2,1,0:T(8,128)(2,1)} %bitcast.81), calls=%async_computation | async-start | bytes 4194304 | tf_op jit(solution)/shard_map/all_to_all | solution.py:314
  191.9 3.5 %fusion.39 = f32[512,512]{0,1:T(8,128)S(1)} fusion(bf16[512,2048]{1,0:T(8,128)(2,1)} %bitcast.75, bf16[2048,256]{1,0:T(8,128)(2,1)} %bitcast.93, bf16[2048,256]{1,0:T(8,128)(2,1)} %bitcast.95), kind=kOutput, calls=%fused_computation.93 | convolution fusion | flops 1077936128 | bytes 5242880 | tf_op jit(solution)/shard_map/dot_general | solution.py:332
  197.0 2.7 collective-permute-start.7
  201.1 2.9 fusion.42
  204.2 2.9 fusion.41
  207.3 30.7 %collective-permute-done.7 = bf16[1024,512]{1,0:T(8,128)(2,1)S(1)} collective-permute-done((bf16[1024,512]{1,0:T(8,128)(2,1)S(1)}, bf16[1024,512]{1,0:T(8,128)(2,1)S(1)}, u32[]{:S(2)}, u32[]{:S(2)}) %collective-permute-start.7) | collective-permute-done | bytes 1048608 | tf_op jit(solution)/shard_map/ppermute | solution.py:328
  240.0 6.0 %convolution_convert_fusion = bf16[512,2048]{1,0:T(8,128)(2,1)} fusion(bf16[1024,2048]{1,0:T(8,128)(2,1)} %constant_dynamic-update-slice_fusion.2, bf16[512,256]{0,1:T(8,128)(2,1)S(1)} %fusion.20, bf16[512,256]{0,1:T(8,128)(2,1)S(1)} %fusion.21, bf16[512,256]{0,1:T(8,128)(2,1)S(1)} %fusion.22, bf16[512,256]{0,1:T(8,128)(2,1)S(1)} %fusion.23), kind=kOutput, calls=%fused_computation.3 | convolution fusion | flops 2152726528 | bytes 7340032 | tf_op jit(solution)/shard_map/dot_general | solution.py:332
  247.3 9.1 %all-to-all-start.2 = ((bf16[32,1,16,2048]{3,2,1,0:T(8,128)(2,1)}), bf16[32,1,16,2048]{3,2,1,0:T(8,128)(2,1)S(1)}, u32[]{:S(2)}, u32[]{:S(2)}) async-start(bf16[32,1,16,2048]{3,2,1,0:T(8,128)(2,1)} %bitcast.82), calls=%async_computation.2 | async-start | bytes 4194304 | tf_op jit(solution)/shard_map/all_to_all | solution.py:368
  256.6 2.9 %reduce_sum.41 = bf16[128,2048]{1,0:T(8,128)(2,1)} reduce(bf16[4,128,2048]{2,1,0:T(8,128)(2,1)} %copy-done.1, bf16[]{:T(256)} %constant.76.clone.1), dimensions={0}, to_apply=%region_0.0 | reduce | flops 786432 | bytes 2621442 | tf_op jit(solution)/shard_map/reduce_sum | solution.py:315
  259.5 25.5 %all-to-all-done.2 = bf16[32,1,16,2048]{3,2,1,0:T(8,128)(2,1)S(1)} async-done(((bf16[32,1,16,2048]{3,2,1,0:T(8,128)(2,1)}), bf16[32,1,16,2048]{3,2,1,0:T(8,128)(2,1)S(1)}, u32[]{:S(2)}, u32[]{:S(2)}) %all-to-all-start.2) | async-done | bytes 2097184 | tf_op jit(solution)/shard_map/all_to_all | solution.py:368
  287.7 3.9 %multiply_reduce_fusion = bf16[128,2048]{1,0:T(8,128)(2,1)} fusion(f32[128,2,2048]{2,1,0:T(2,128)S(1)} %reshape.120, f32[128,2]{1,0:T(8,128)S(1)} %copy.61), kind=kLoop, calls=%fused_computation.6 | loop fusion | flops 786432 | bytes 2622464 | tf_op jit(solution)/shard_map/reduce_sum | solution.py:371
  (108 shorter events, 42.5 us)
Async XLA Ops:
  0.6 46.9 %copy-start = (f32[16384,4]{0,1:T(4,128)S(1)}, f32[16384,4]{0,1:T(4,128)}, u32[]{:S(2)}) copy-start(f32[16384,4]{0,1:T(4,128)} %param.15) | copy-start | bytes 786436
  0.6 5.3 %copy-start.7 = (bf16[512,256]{1,0:T(8,128)(2,1)S(1)}, bf16[512,256]{1,0:T(8,128)(2,1)}, u32[]{:S(2)}) copy-start(bf16[512,256]{1,0:T(8,128)(2,1)} %param.14) | copy-start | bytes 786436
  0.7 151.1 %collective-permute-start.8 = (bf16[256,2048]{1,0:T(8,128)(2,1)}, bf16[256,2048]{1,0:T(8,128)(2,1)S(1)}, u32[]{:S(2)}, u32[]{:S(2)}) collective-permute-start(bf16[256,2048]{1,0:T(8,128)(2,1)} %bitcast.87), channel_id=1, source_target_pairs={{0,1},{1,2},{2,3},{3,0},{4,5},{5,6},{6,7},{7,4},{8,9},{9,10},{10,1... | collective-permute-start | bytes 3145736 | tf_op jit(solution)/shard_map/ppermute | solution.py:323
  2.8 156.7 %collective-permute-start.9 = (bf16[256,2048]{1,0:T(8,128)(2,1)}, bf16[256,2048]{1,0:T(8,128)(2,1)}, u32[]{:S(2)}, u32[]{:S(2)}) collective-permute-start(bf16[256,2048]{1,0:T(8,128)(2,1)} %bitcast.88), channel_id=1, source_target_pairs={{0,3},{1,0},{2,1},{3,2},{4,7},{5,4},{6,5},{7,6},{8,11},{9,8},{10,9... | collective-permute-start | bytes 3145736 | tf_op jit(solution)/shard_map/ppermute | solution.py:323
  77.1 27.1 %copy-start.6 = (bf16[2,64,512]{2,1,0:T(8,128)(2,1)S(1)}, bf16[2,64,512]{2,1,0:T(8,128)(2,1)}, u32[]{:S(2)}) copy-start(bf16[2,64,512]{2,1,0:T(8,128)(2,1)} %stick_attend.2) | copy-start | bytes 393220
  77.1 30.9 %copy-start.10 = (s32[128,2]{0,1:T(2,128)S(1)}, s32[128,2]{0,1:T(2,128)}, u32[]{:S(2)}) copy-start(s32[128,2]{0,1:T(2,128)} %param.19) | copy-start | bytes 3076
  103.2 6.3 %copy-start.4 = (bf16[128,2048]{1,0:T(8,128)(2,1)S(1)}, bf16[128,2048]{1,0:T(8,128)(2,1)}, u32[]{:S(2)}) copy-start(bf16[128,2048]{1,0:T(8,128)(2,1)} %param.17) | copy-start | bytes 1572868
  103.2 6.6 %copy-start.9 = (f32[2048]{0:T(1024)S(1)}, f32[2048]{0:T(1024)}, u32[]{:S(2)}) copy-start(f32[2048]{0:T(1024)} %param.18) | copy-start | bytes 24580
  105.8 20.3 %collective-permute-start = (bf16[64,512]{1,0:T(8,128)(2,1)}, bf16[64,512]{1,0:T(8,128)(2,1)}, u32[]{:S(2)}, u32[]{:S(2)}) collective-permute-start(bf16[64,512]{1,0:T(8,128)(2,1)} %get-tuple-element.10), channel_id=1, source_target_pairs={{0,0},{4,4},{32,8},{36,12},{64,16},{68,20},{96,24},{100,28},{108,3... | collective-permute-start | bytes 196616 | tf_op jit(solution)/shard_map/ppermute | solution.py:309
  114.8 72.2 %all-to-all-start.1 = ((bf16[32,1,16,2048]{3,2,1,0:T(8,128)(2,1)}), bf16[32,1,16,2048]{3,2,1,0:T(8,128)(2,1)S(1)}, u32[]{:S(2)}, u32[]{:S(2)}) async-start(bf16[32,1,16,2048]{3,2,1,0:T(8,128)(2,1)} %bitcast.27), calls=%async_computation.1 | async-start | bytes 4194304 | tf_op jit(solution)/shard_map/all_to_all | solution.py:353
  121.6 10.2 %copy-start.5 = (bf16[1,256,2048]{2,1,0:T(8,128)(2,1)S(1)}, bf16[1,256,2048]{2,1,0:T(8,128)(2,1)}, u32[]{:S(2)}) copy-start(bf16[1,256,2048]{2,1,0:T(8,128)(2,1)} %param.23) | copy-start | bytes 3145732
  124.7 70.9 %collective-permute-start.5 = (bf16[2048,512]{1,0:T(8,128)(2,1)}, bf16[2048,512]{1,0:T(8,128)(2,1)}, u32[]{:S(2)}, u32[]{:S(2)}) collective-permute-start(bf16[2048,512]{1,0:T(8,128)(2,1)} %pad_maximum_fusion), channel_id=1, source_target_pairs={{0,3},{1,0},{2,1},{3,2},{4,7},{5,4},{6,5},{7,6},{8,11},{9,8},{10,9... | collective-permute-start | bytes 6291464 | tf_op jit(solution)/shard_map/ppermute | solution.py:323
  126.0 73.8 %collective-permute-start.4 = (bf16[2048,512]{1,0:T(8,128)(2,1)}, bf16[2048,512]{1,0:T(8,128)(2,1)}, u32[]{:S(2)}, u32[]{:S(2)}) collective-permute-start(bf16[2048,512]{1,0:T(8,128)(2,1)} %pad_maximum_fusion), channel_id=1, source_target_pairs={{0,1},{1,2},{2,3},{3,0},{4,5},{5,6},{6,7},{7,4},{8,9},{9,10},{10,1... | collective-permute-start | bytes 6291464 | tf_op jit(solution)/shard_map/ppermute | solution.py:323
  126.2 21.9 %collective-permute-start.1 = (bf16[64,512]{1,0:T(8,128)(2,1)}, bf16[64,512]{1,0:T(8,128)(2,1)}, u32[]{:S(2)}, u32[]{:S(2)}) collective-permute-start(bf16[64,512]{1,0:T(8,128)(2,1)} %get-tuple-element.13), channel_id=1, source_target_pairs={{8,0},{12,4},{40,8},{44,12},{72,16},{76,20},{104,24},{108,28},{116... | collective-permute-start | bytes 196616 | tf_op jit(solution)/shard_map/ppermute | solution.py:309
  148.1 6.7 %collective-permute-start.2 = (bf16[64,512]{1,0:T(8,128)(2,1)S(1)}, bf16[64,512]{1,0:T(8,128)(2,1)S(1)}, u32[]{:S(2)}, u32[]{:S(2)}) collective-permute-start(bf16[64,512]{1,0:T(8,128)(2,1)S(1)} %get-tuple-element.12), channel_id=1, source_target_pairs={{16,0},{20,4},{48,8},{52,12},{80,16},{84,20},{112,24},{116,28},{12... | collective-permute-start | bytes 196616 | tf_op jit(solution)/shard_map/ppermute | solution.py:309
  151.8 4.7 %collective-permute-start.3 = (bf16[64,512]{1,0:T(8,128)(2,1)S(1)}, bf16[64,512]{1,0:T(8,128)(2,1)S(1)}, u32[]{:S(2)}, u32[]{:S(2)}) collective-permute-start(bf16[64,512]{1,0:T(8,128)(2,1)S(1)} %get-tuple-element.11), channel_id=1, source_target_pairs={{24,0},{28,4},{56,8},{60,12},{88,16},{92,20},{120,24},{124,28},{10... | collective-permute-start | bytes 196616 | tf_op jit(solution)/shard_map/ppermute | solution.py:309
  154.8 30.5 %collective-permute-start.10 = (bf16[128,2048]{1,0:T(8,128)(2,1)S(1)}, bf16[128,2048]{1,0:T(8,128)(2,1)S(1)}, u32[]{:S(2)}, u32[]{:S(2)}) collective-permute-start(bf16[128,2048]{1,0:T(8,128)(2,1)S(1)} %slice.107), channel_id=1, source_target_pairs={{0,1},{1,2},{2,3},{3,0},{4,5},{5,6},{6,7},{7,4},{8,9},{9,10},{10,1... | collective-permute-start | bytes 1572872 | tf_op jit(solution)/shard_map/ppermute | solution.py:328
  160.5 25.6 %collective-permute-start.11 = (bf16[128,2048]{1,0:T(8,128)(2,1)S(1)}, bf16[128,2048]{1,0:T(8,128)(2,1)S(1)}, u32[]{:S(2)}, u32[]{:S(2)}) collective-permute-start(bf16[128,2048]{1,0:T(8,128)(2,1)S(1)} %slice.108), channel_id=1, source_target_pairs={{0,3},{1,0},{2,1},{3,2},{4,7},{5,4},{6,5},{7,6},{8,11},{9,8},{10,9... | collective-permute-start | bytes 1572872 | tf_op jit(solution)/shard_map/ppermute | solution.py:328
  188.3 57.7 %all-to-all-start = ((bf16[4,128,2048]{2,1,0:T(8,128)(2,1)}), bf16[4,128,2048]{2,1,0:T(8,128)(2,1)S(1)}, u32[]{:S(2)}, u32[]{:S(2)}) async-start(bf16[4,128,2048]{2,1,0:T(8,128)(2,1)} %bitcast.81), calls=%async_computation | async-start | bytes 4194304 | tf_op jit(solution)/shard_map/all_to_all | solution.py:314
  195.5 5.6 %copy-start.3 = (bf16[32,1,16,2048]{3,2,1,0:T(8,128)(2,1)S(1)}, bf16[32,1,16,2048]{3,2,1,0:T(8,128)(2,1)}, u32[]{:S(2)}) copy-start(bf16[32,1,16,2048]{3,2,1,0:T(8,128)(2,1)} %copy-done.2) | copy-start | bytes 6291460
  197.0 40.9 %collective-permute-start.7 = (bf16[1024,512]{1,0:T(8,128)(2,1)S(1)}, bf16[1024,512]{1,0:T(8,128)(2,1)S(1)}, u32[]{:S(2)}, u32[]{:S(2)}) collective-permute-start(bf16[1024,512]{1,0:T(8,128)(2,1)S(1)} %slice.104), channel_id=1, source_target_pairs={{0,3},{1,0},{2,1},{3,2},{4,7},{5,4},{6,5},{7,6},{8,11},{9,8},{10,9... | collective-permute-start | bytes 3145736 | tf_op jit(solution)/shard_map/ppermute | solution.py:328
  201.0 38.1 %collective-permute-start.6 = (bf16[1024,512]{1,0:T(8,128)(2,1)S(1)}, bf16[1024,512]{1,0:T(8,128)(2,1)S(1)}, u32[]{:S(2)}, u32[]{:S(2)}) collective-permute-start(bf16[1024,512]{1,0:T(8,128)(2,1)S(1)} %slice.102), channel_id=1, source_target_pairs={{0,1},{1,2},{2,3},{3,0},{4,5},{5,6},{6,7},{7,4},{8,9},{9,10},{10,1... | collective-permute-start | bytes 3145736 | tf_op jit(solution)/shard_map/ppermute | solution.py:328
  246.0 10.4 %copy-start.11 = (f32[128,2]{0,1:T(2,128)S(1)}, f32[128,2]{0,1:T(2,128)}, u32[]{:S(2)}) copy-start(f32[128,2]{0,1:T(2,128)} %param.20) | copy-start | bytes 3076
  247.3 37.6 %all-to-all-start.2 = ((bf16[32,1,16,2048]{3,2,1,0:T(8,128)(2,1)}), bf16[32,1,16,2048]{3,2,1,0:T(8,128)(2,1)S(1)}, u32[]{:S(2)}, u32[]{:S(2)}) async-start(bf16[32,1,16,2048]{3,2,1,0:T(8,128)(2,1)} %bitcast.82), calls=%async_computation.2 | async-start | bytes 4194304 | tf_op jit(solution)/shard_map/all_to_all | solution.py:368
  (3 other events, 3.9 us)

commit v3 on v1

v3 whole, which is shorter than its diff:
```python
import math

import jax
import jax.numpy as jnp
from jax import lax
from jax.experimental import pallas as pl
from jax.experimental.pallas import tpu as pltpu
from jax.sharding import PartitionSpec as P


HEAD_DIM = 64
GROUPS = 4
TOPK = 2
BLOCK = 512
HALF = 256
RUNS = 8
RUN = HALF // RUNS
LOG2E = math.log2(math.e)
U_CAP = 48.0
MESH = pl.DeviceIdType.MESH
norm_eps = 1e-06


def turn_of(block):
    slot, at = block // 8, block % 8
    return jnp.where(slot % 2 == 0, at, 7 - at)


def block_of(slot, turn):
    return slot * 8 + jnp.where(slot % 2 == 0, turn, 7 - turn)


def mix_kernel(
    kv_ref, q_ref, rows_ref, rows_out_ref, home_ref, rows_in_ref,
    kv_all, qt_ref, done_ref, kk_ref, bias_ref, rhs_ref, z_hi, z_lo, w_hi, w_lo, acc_ref, carry_ref,
    got, q_got, home_got, row_got, s_col, s_up, s_down, s_pair, s_q, s_home, s_row, s_own,
):
    me = lax.axis_index("ep")
    z, y, c = me // 8, me // 2 % 4, me % 2
    turn = 2 * z + c
    my_turn = turn_of(me)
    lanes = qt_ref.shape[2]

    def at(zz, yy, cc):
        return (zz + 4) % 4 * 8 + (yy + 4) % 4 * 2 + cc

    def dest(index):
        return {"ep": index}

    def q_dest(h):
        return my_turn // 2 * 8 + 2 * h + my_turn % 2

    barrier = pltpu.get_barrier_semaphore()

    def greet(d, carried):
        pl.semaphore_signal(barrier, inc=1, device_id=dest((me + d) % 32), device_id_type=MESH)
        return carried

    lax.fori_loop(1, 32, greet, 0)
    pl.semaphore_wait(barrier, 31)

    def send(src, index, dst, send_sem, recv_sem):
        copy = pltpu.make_async_remote_copy(
            src_ref=src, dst_ref=dst, send_sem=send_sem, recv_sem=recv_sem,
            device_id=dest(index), device_id_type=MESH,
        )
        copy.start()
        return copy

    def piece(index):
        return kv_all.at[index]

    def arrived(index):
        pltpu.make_async_copy(piece(index), piece(index), got.at[index]).wait()

    sent = []
    for d in (1, 2, 3):
        sent.append(send(kv_ref.at[(y + d) % 4], at(z, y + d, c), piece(me), s_col.at[d - 1], got.at[me]))
    for h in range(4):
        @pl.when(q_dest(h) != me)
        def _():
            send(q_ref.at[h], q_dest(h), qt_ref.at[z], s_q.at[h], q_got.at[z])

        @pl.when(q_dest(h) == me)
        def _():
            pltpu.make_async_copy(q_ref.at[h], qt_ref.at[z], q_got.at[z]).start()
    own = pltpu.make_async_copy(kv_ref.at[y], piece(me), s_own.at[0])
    own.start()
    for d in range(4):
        index = at(z, y - d, c)
        if d > 0:
            arrived(index)
        src = kv_ref.at[y] if d == 0 else piece(index)
        sent.append(send(src, at(z + 1, y, c), piece(index), s_up.at[d], got.at[index]))
        sent.append(send(src, at(z - 1, y, c), piece(index), s_down.at[d], got.at[index]))
        sent.append(send(src, at(z, y, 1 - c), piece(index), s_pair.at[d], got.at[index]))

    low_lane = lax.broadcasted_iota(jnp.int32, (HALF, 128), 1) < HEAD_DIM
    sub = lax.broadcasted_iota(jnp.int32, (RUNS, 128), 0)
    row = lax.broadcasted_iota(jnp.int32, (128, lanes), 0)

    def build_bias(b, carried):
        for half in range(2):
            value = rows_ref[b, half : half + 1, :] * LOG2E
            parts = jnp.zeros((128, HALF), jnp.float32)
            for n in range(3):
                part = value.astype(jnp.bfloat16).astype(jnp.float32)
                parts = jnp.where(row[:, 0:HALF] == n, part, parts)
                value = value - part
            bias_ref[b, half] = parts.T.astype(jnp.bfloat16)
        return carried

    lax.fori_loop(0, 32, build_bias, 0)

    for d in range(4):
        for n, dz in enumerate((1, -1)):
            index = at(z - dz, y - d, c)
            arrived(index)
            if d < 2 and dz == 1:
                sent.append(send(piece(index), at(z + 1, y, c), piece(index), s_up.at[4 + d], got.at[index]))
            if d >= 2 and dz == -1:
                sent.append(send(piece(index), at(z - 1, y, c), piece(index), s_down.at[2 + d], got.at[index]))
            sent.append(send(piece(index), at(z, y, 1 - c), piece(index), s_pair.at[4 + 2 * d + n], got.at[index]))
    for d in (0, 2, 1, 3):
        index = at(z + 2, y - d, c)
        arrived(index)
        sent.append(send(piece(index), at(z, y, 1 - c), piece(index), s_pair.at[12 + d], got.at[index]))

    def depart(d, carried):
        index = (me + d) % 32
        send(rows_out_ref.at[index], index, rows_in_ref.at[me], s_row.at[index], row_got.at[me])
        return carried

    lax.fori_loop(1, 32, depart, 0)
    mine = pltpu.make_async_copy(rows_out_ref.at[me], rows_in_ref.at[me], s_own.at[1])
    mine.start()

    for k in range(4):
        pltpu.make_async_copy(qt_ref.at[k], qt_ref.at[k], q_got.at[k]).wait()
    for zz in range(4):
        for yy in range(4):
            arrived(at(zz, yy, 1 - c))
    own.wait()

    def build(b, carried):
        pair = kv_all[b, 0:HALF, :].astype(jnp.float32)
        turned = pltpu.roll(pair, HEAD_DIM, axis=1)
        kk_ref[b, 0] = jnp.where(low_lane, pair, turned).astype(jnp.bfloat16)
        kk_ref[b, 1] = jnp.where(low_lane, turned, pair).astype(jnp.bfloat16)
        return carried

    lax.fori_loop(0, 32, build, 0)

    def later(x, n):
        return jnp.where(sub < RUNS - n, pltpu.roll(x, RUNS - n, axis=0), 1.0)

    def scores(b, half, z_ref):
        keys = jnp.concatenate([kk_ref[b, half], bias_ref[b, half]], axis=1)
        z_ref[...] = jnp.dot(keys, rhs_ref[...], preferred_element_type=jnp.float32)

    def weigh(z_ref, w_ref, first_key):
        for lane in range(0, lanes, 128):
            ls = slice(lane, lane + 128)
            us = []
            for i in range(RUN):
                u = jnp.exp2(jnp.minimum(z_ref[RUNS * i : RUNS * i + RUNS, ls], U_CAP))
                if first_key is not None:
                    query = lax.broadcasted_iota(jnp.int32, (RUNS, 128), 1) + lane
                    u = jnp.where(sub * RUN + (i + first_key) < query, u, 0.0)
                us.append(u)
            pairs = range(RUN // 2)
            rs = [1.0 / ((1.0 + us[2 * g]) * (1.0 + us[2 * g + 1])) for g in pairs]
            tree = list(rs)
            while len(tree) > 1:
                tree = [tree[2 * n] * tree[2 * n + 1] for n in range(len(tree) // 2)]
            total = tree[0]
            after = later(total, 1)
            after = after * later(after, 1)
            after = after * later(after, 2)
            after = after * later(after, 4)
            carry = carry_ref[:, ls]
            left = carry * after
            carry_ref[:, ls] = carry * jnp.broadcast_to((after * total)[0:1, :], (RUNS, 128))
            for g in reversed(pairs):
                left = left * rs[g]
                first = us[2 * g] * left
                second = us[2 * g + 1] * (left * (1.0 + us[2 * g]))
                both = jnp.concatenate([first, second], axis=0)
                w_ref[2 * RUNS * g : 2 * RUNS * g + 2 * RUNS, ls] = both.astype(jnp.bfloat16)

    def collect(b, half, w_ref):
        first = HALF + 2 * HEAD_DIM * half
        values = jnp.concatenate(
            [kv_all[b, first : first + HEAD_DIM, :], kv_all[b, first + HEAD_DIM : first + 2 * HEAD_DIM, :]], axis=1
        )
        acc_ref[...] += jnp.dot(values, w_ref[...], preferred_element_type=jnp.float32)

    def tile(n, carried):
        p = block_of(n, turn)
        scaled = qt_ref[n].astype(jnp.float32) * (LOG2E * HEAD_DIM**-0.5)
        top = scaled.astype(jnp.bfloat16)
        rhs_ref[0:HEAD_DIM, :] = top
        rhs_ref[HEAD_DIM : 2 * HEAD_DIM, :] = (scaled - top.astype(jnp.float32)).astype(jnp.bfloat16)
        rhs_ref[128:256, :] = jnp.where(row < 3, 1.0, 0.0).astype(jnp.bfloat16)
        carry_ref[...] = jnp.ones_like(carry_ref)
        acc_ref[...] = jnp.zeros_like(acc_ref)
        scores(p, 1, z_hi)
        scores(p, 0, z_lo)
        weigh(z_hi, w_hi, HALF)
        scores(jnp.maximum(p - 1, 0), 1, z_hi)
        weigh(z_lo, w_lo, 0)
        collect(p, 1, w_hi)

        def visit(step, inner):
            b = p - 1 - step
            scores(b, 0, z_lo)
            weigh(z_hi, w_hi, None)
            collect(b + 1, 0, w_lo)
            scores(jnp.maximum(b - 1, 0), 1, z_hi)
            weigh(z_lo, w_lo, None)
            collect(b, 1, w_hi)
            return inner

        lax.fori_loop(0, p, visit, 0)
        collect(0, 0, w_lo)
        done_ref[n] = acc_ref[...].astype(jnp.bfloat16)
        return carried

    lax.fori_loop(0, 4, tile, 0)

    for n in range(4):
        @pl.when(block_of(n, turn) != me)
        def _():
            send(done_ref.at[n], block_of(n, turn), home_ref.at[y], s_home.at[n], home_got.at[y])

        @pl.when(block_of(n, turn) == me)
        def _():
            pltpu.make_async_copy(done_ref.at[n], home_ref.at[y], home_got.at[y]).start()
    for h in range(4):
        pltpu.make_async_copy(home_ref.at[h], home_ref.at[h], home_got.at[h]).wait()

    def land(d, carried):
        index = (me + d) % 32
        pltpu.make_async_copy(rows_in_ref.at[index], rows_in_ref.at[index], row_got.at[index]).wait()
        pltpu.make_async_copy(rows_out_ref.at[index], rows_out_ref.at[index], s_row.at[index]).wait()
        return carried

    lax.fori_loop(1, 32, land, 0)
    mine.wait()
    for copy in sent:
        copy.wait_send()
    for h in range(4):
        @pl.when(q_dest(h) != me)
        def _():
            pltpu.make_async_copy(q_ref.at[h], q_ref.at[h], s_q.at[h]).wait()

        @pl.when(block_of(h, turn) != me)
        def _():
            pltpu.make_async_copy(done_ref.at[h], done_ref.at[h], s_home.at[h]).wait()


def mix(kv, q, bias, rows):
    whole = pl.BlockSpec(memory_space=pltpu.VMEM)
    anywhere = pl.BlockSpec(memory_space=pl.ANY)
    dma = pltpu.SemaphoreType.DMA
    bf16, f32 = jnp.bfloat16, jnp.float32
    return pl.pallas_call(
        mix_kernel,
        out_shape=(jax.ShapeDtypeStruct(q.shape, bf16), jax.ShapeDtypeStruct(rows.shape, bf16)),
        in_specs=[whole, whole, whole, anywhere],
        out_specs=(whole, anywhere),
        scratch_shapes=[
            pltpu.VMEM((32,) + kv.shape[1:], bf16),
            pltpu.VMEM(q.shape, bf16),
            pltpu.VMEM(q.shape, bf16),
            pltpu.VMEM((32, 2, HALF, 128), bf16),
            pltpu.VMEM((32, 2, HALF, 128), bf16),
            pltpu.VMEM((HALF, BLOCK), bf16),
            pltpu.VMEM((HALF, BLOCK), f32),
            pltpu.VMEM((HALF, BLOCK), f32),
            pltpu.VMEM((HALF, BLOCK), bf16),
            pltpu.VMEM((HALF, BLOCK), bf16),
            pltpu.VMEM((HEAD_DIM, BLOCK), f32),
            pltpu.VMEM((RUNS, BLOCK), f32),
            dma((32,)), dma((4,)), dma((4,)), dma((32,)),
            dma((3,)), dma((6,)), dma((6,)), dma((16,)), dma((4,)), dma((4,)), dma((32,)), dma((2,)),
        ],
        compiler_params=pltpu.CompilerParams(collective_id=1, has_side_effects=True),
        cost_estimate=pl.CostEstimate(flops=60_000_000_000, bytes_accessed=12 << 20, transcendentals=0),
        name="mix",
    )(kv, q, bias, rows)


def key_order(rows):
    n = rows.shape[-1]
    return rows.reshape(2, RUNS, RUN, n).swapaxes(1, 2).reshape(BLOCK, n)


def route(expert_pick, expert_total, capacity):
    picks = expert_pick.reshape(-1)
    matches = (picks[:, None] == jnp.arange(expert_total, dtype=jnp.int32)[None, :]).astype(jnp.int32)
    ranks = jnp.sum((jnp.cumsum(matches, axis=0) - matches) * matches, axis=1)
    return picks * capacity + ranks


def dot(a, b):
    return jnp.dot(a, b, preferred_element_type=jnp.float32)


def local(
    query_rows, key_rows, value_rows, key_bias, out_weight, moe_input, moe_gain,
    expert_pick, route_weight, w_gate, w_up, w_down,
):
    ep_index = lax.axis_index("ep")
    ep_count = lax.axis_size("ep")
    head = (ep_index >> 1) & 3
    token_count, width = moe_input.shape
    capacity = GROUPS * token_count // ep_count

    gates = lax.all_gather(w_gate[0], "tp")
    ups = lax.all_gather(w_up[0], "tp")
    downs = lax.all_gather(w_down[0], "tp", axis=0, tiled=True)

    q_heads = query_rows.T.reshape(4, HEAD_DIM, BLOCK)
    keys = key_order(key_rows).reshape(2, HALF, 4, HEAD_DIM)
    k_heads = keys.transpose(2, 1, 0, 3).reshape(4, HALF, 128)
    values = key_order(value_rows).T.reshape(4, HEAD_DIM, 4, 128)
    v_heads = values.transpose(0, 2, 1, 3).reshape(4, HALF, 128)
    kv = jnp.concatenate([k_heads, v_heads], axis=1)
    column = lax.dynamic_slice_in_dim(key_bias, head, 1, 1)
    bias = column.reshape(32, 2, RUNS, RUN).swapaxes(2, 3).reshape(32, 2, HALF)

    widened = moe_input.astype(jnp.float32)
    normed = (
        widened * lax.rsqrt(jnp.mean(widened * widened, axis=1, keepdims=True) + norm_eps) * moe_gain
    ).astype(jnp.bfloat16)
    slots = route(expert_pick, ep_count, capacity)
    owners = jnp.arange(slots.shape[0], dtype=jnp.int32) // TOPK
    table = jnp.full((ep_count * capacity,), token_count, jnp.int32).at[slots].set(owners)
    padded = jnp.concatenate([normed, jnp.zeros((1, width), jnp.bfloat16)], axis=0)
    outgoing = padded[table].reshape(ep_count, capacity, width)

    home, arrived = mix(kv, q_heads, bias, outgoing)

    part = jnp.einsum("cr,cm->rm", home.reshape(4 * HEAD_DIM, BLOCK), out_weight, preferred_element_type=jnp.float32)
    pieces = part.astype(jnp.bfloat16).reshape(4, 128, width)
    summed = lax.all_to_all(pieces, "tp", split_axis=0, concat_axis=0, tiled=True)
    mixer_out = summed.astype(jnp.float32).sum(axis=0).astype(jnp.bfloat16)

    rows = arrived.reshape(ep_count * capacity, width)
    gate_in = jnp.einsum("tm,smf->tsf", rows, gates, preferred_element_type=jnp.float32)
    up_in = jnp.einsum("tm,smf->tsf", rows, ups, preferred_element_type=jnp.float32)
    hidden = (jax.nn.silu(gate_in) * up_in).astype(jnp.bfloat16).reshape(rows.shape[0], -1)
    served = dot(hidden, downs).astype(jnp.bfloat16).reshape(ep_count, capacity, width)
    returned = lax.all_to_all(served, "ep", split_axis=0, concat_axis=0, tiled=True)
    flat = returned.reshape(ep_count * capacity, width)
    chosen = flat[slots].reshape(token_count, TOPK, width).astype(jnp.float32)
    routed_out = jnp.sum(chosen * route_weight[:, :, None], axis=1).astype(jnp.bfloat16)
    return (mixer_out, routed_out)


def solution(mesh):
    placed = (
        P("ep", "tp"), P("ep", "tp"), P("ep", "tp"), P(None, "tp"), P("tp", None),
        P(("ep", "tp"), None), P(), P(("ep", "tp"), None), P(("ep", "tp"), None),
        P("ep", None, "tp"), P("ep", None, "tp"), P("ep", "tp", None),
    )
    return jax.shard_map(
        local,
        mesh=mesh,
        in_specs=placed,
        out_specs=(P(("ep", "tp"), None), P(("ep", "tp"), None)),
        check_vma=False,
    )
```

time: 225 us -> 244 us (1.084)
  Pallas kernels: 44.5 us -> 83.4 us
  starting transfers between devices: 48.5 us -> 23.3 us
  waiting for transfers between devices: 54.4 us -> 74.2 us
  other arithmetic: 19.5 us -> 8.82 us
  local copies, waits for them, and re-layouts: 21.9 us -> 16.1 us
  matrix products: 20.2 us -> 23 us
    pallas_call x1, Pallas kernels: 44.5 us -> 83.4 us  [mix(): pl.pallas_call(mix_kernel, out_shape=(jax.ShapeDtypeStruct(q.shape, bf16)...]
    all_gather x2 -> x3, waiting for transfers between devices: 8.64 us -> 46.6 us  [the longest x1 46.6 us: local(): downs = lax.all_gather(w_down[0], 'tp', axis=0, tiled=True)]
    ppermute x8 -> x0, waiting for transfers between devices: 29.7 us -> none  [the longest x4 23.7 us: mixer(): q_got.append(lax.ppermute(mine, 'ep', routes(r)))]
    ppermute x8 -> x0, starting transfers between devices: 17.2 us -> none  [the longest x4 8.85 us: mixer(): q_got.append(lax.ppermute(mine, 'ep', routes(r)))]
    all_to_all x4 -> x2, waiting for transfers between devices: 16 us -> 25.5 us  [the longest x1 25.5 us: local(): lax.all_to_all(served, 'ep', split_axis=0, concat_axis=0, tiled=True)]
    convert_element_type x3 -> x2, other arithmetic: 8.82 us -> 0.2 us  [the longest x1 0.19 us: local(): normed = (widened * lax.rsqrt(jnp.mean(widened * widened, axis=1, keepdim...]
    all_to_all x4 -> x2, starting transfers between devices: 31.2 us -> 23.1 us  [the longest x1 19.1 us: local(): lax.all_to_all(served, 'ep', split_axis=0, concat_axis=0, tiled=True)]
    convert_element_type x2 -> x1, local copies, waits for them, and re-layouts: 5.44 us -> 2.37 us  [local(): chosen = flat[slots].reshape(token_count, TOPK, width).astype(jnp.float32)]
  transfers between devices with their start and end apart: 14 -> 5, of which waited for: 8 -> 2; matrix products, arithmetic and copies ran while one was open for 22% -> 16% of each run, Pallas kernels for 20% -> 34%
where the time goes in v3:
time: 244 us; the launch traced here: 243 us
  Pallas kernels  83.4 us (34%)
  waiting for transfers between devices  74.2 us (30%)
  starting transfers between devices  23.3 us (10%)
  matrix products  23 us (9%)
  local copies, waits for them, and re-layouts  16.1 us (7%)
  between operations  14 us (6%)
  other arithmetic  8.82 us (4%)
    pallas_call x1, Pallas kernels, mix(): pl.pallas_call(mix_kernel, out_shape=(jax.ShapeDtypeStruct(q.shape, bf16)...  83.4 us
    all_gather x1, waiting for transfers between devices, local(): downs = lax.all_gather(w_down[0], 'tp', axis=0, tiled=True)  46.6 us
    all_to_all x1, waiting for transfers between devices, local(): lax.all_to_all(served, 'ep', split_axis=0, concat_axis=0, tiled=True)  25.5 us
    all_to_all x1, starting transfers between devices, local(): lax.all_to_all(served, 'ep', split_axis=0, concat_axis=0, tiled=True)  19.1 us
    dot_general x1, matrix products, local(): jnp.einsum('tm,smf->tsf', rows, gates, preferred_element_type=jnp.float32)  7.23 us
    dot_general x1, matrix products, local(): jnp.einsum('tm,smf->tsf', rows, ups, preferred_element_type=jnp.float32)  6.55 us
    dot_general x1, matrix products, dot(): return jnp.dot(a, b, preferred_element_type=jnp.float32)  6.21 us
  transfers between devices with their start and end apart: 5, of which 2 were waited for; matrix products, arithmetic and copies ran while one was open for 16% of the time, Pallas kernels for 34%

profile of v3, /device:TPU:1, one launch (start us, length us, event | category | flops | bytes accessed | tf_op | source)
XLA Modules:
  0.0 242.8 jit_solution(1256089799476488690)
XLA Ops:
  7.2 0.7 all-gather.7.cloned.1.call-update
  8.0 0.7 all-gather.5.cloned.1.call-update
  8.7 0.7 all-gather.9.cloned.1.call-update
  9.9 0.6 reduce-window.6
  11.1 1.4 scatter_custom_fusion
  12.7 1.2 dynamic-slice_reduce_fusion
  14.2 0.7 copy.61.rows_ref
  16.3 0.8 copy.55
  17.4 3.3 %gather_fusion = bf16[512,2048]{1,0:T(8,128)(2,1)} fusion(bf16[129,2048]{1,0:T(8,128)(2,1)S(1)} %concatenate.7, s32[1024]{0:T(1024)S(1)} %pad_clamp_fusion.1), kind=kCustom, calls=%fused_computation | custom fusion | bytes 4196352 | tf_op jit(solution)/shard_map/gather | solution.py:341
  20.7 0.8 pad_maximum_fusion.kv_ref
  21.5 83.4 %mix.1 = (bf16[4,64,512]{2,1,0:T(8,128)(2,1)}, bf16[32,16,2048]{2,1,0:T(8,128)(2,1)}) custom-call(bf16[4,512,128]{2,1,0:T(8,128)(2,1)} %pad_maximum_fusion.kv_ref, bf16[4,64,512]{2,1,0:T(8,128)(2,1)} %bitcast.77, f32[32,2,256]{2,1,0:T(2,128)} %copy.61.rows_ref, bf16[32,16,2048]{2,1,0:T(8,128)(2,1)} %bitcast.63), custom_call_target="tpu_custom_call" | custom-call | flops 60000002048 | bytes 12582912 | tf_op jit(solution)/shard_map/mix/pallas_call | solution.py:267
  104.9 3.0 %convolution_convert_fusion = bf16[512,2048]{1,0:T(8,128)(2,1)} fusion(bf16[256,512]{1,0:T(8,128)(2,1)} %bitcast.73, bf16[256,2048]{1,0:T(8,128)(2,1)S(1)} %copy-done), kind=kOutput, calls=%fused_computation.6 | convolution fusion | flops 537919488 | bytes 3407872 | tf_op jit(solution)/shard_map/cr,cm->rm/dot_general | solution.py:345
  107.9 4.0 %all-to-all-start = ((bf16[4,128,2048]{2,1,0:T(8,128)(2,1)}), bf16[4,128,2048]{2,1,0:T(8,128)(2,1)S(1)}, u32[]{:S(2)}, u32[]{:S(2)}) async-start(bf16[4,128,2048]{2,1,0:T(8,128)(2,1)} %bitcast.19), calls=%async_computation | async-start | bytes 4194304 | tf_op jit(solution)/shard_map/all_to_all | solution.py:347
  112.0 6.5 %fusion.14 = f32[512,4,256]{0,2,1:T(8,128)} fusion(bf16[512,2048,1]{1,0,2:T(8,128)(2,1)} %bitcast.81, bf16[4,2048,256]{2,1,0:T(8,128)(2,1)} %all-gather.7.cloned.1.call-done), kind=kOutput, calls=%fused_computation.38 | convolution fusion | flops 2147483648 | bytes 8388608 | tf_op jit(solution)/shard_map/tm,smf->tsf/dot_general | solution.py:352
  118.5 7.2 %multiply_convert_fusion = bf16[512,4,256]{0,2,1:T(8,128)(2,1)} fusion(f32[512,4,256]{0,2,1:T(8,128)} %fusion.14, bf16[512,2048,1]{1,0,2:T(8,128)(2,1)} %bitcast.82, bf16[4,2048,256]{2,1,0:T(8,128)(2,1)} %all-gather.5.cloned.1.call-done), kind=kOutput, calls=%fused_computation.8 | convolution fusion | flops 2150629376 | bytes 9437184 | tf_op jit(solution)/shard_map/tm,smf->tsf/dot_general | solution.py:351
  125.7 46.6 %all-gather.9.cloned.1.call-done = bf16[1,1024,2048]{2,1,0:T(8,128)(2,1)} async-done(((bf16[1,256,2048]{2,1,0:T(8,128)(2,1)}), bf16[1,1024,2048]{2,1,0:T(8,128)(2,1)}) %all-gather.9.cloned.1.call-update) | async-done | bytes 4194320 | tf_op jit(solution)/shard_map/all_gather | solution.py:322
  172.4 6.2 %fusion.2 = bf16[512,2048]{1,0:T(8,128)(2,1)} fusion(bf16[512,1024]{0,1:T(8,128)(2,1)} %bitcast.83, bf16[1,1024,2048]{2,1,0:T(8,128)(2,1)} %all-gather.9.cloned.1.call-done), kind=kOutput, calls=%fused_computation.5 | convolution fusion | flops 2148532224 | bytes 7340032 | tf_op jit(solution)/shard_map/dot_general | solution.py:307
  178.6 1.3 copy-done.1
  180.0 19.1 %all-to-all-start.1 = ((bf16[32,16,2048]{2,1,0:T(8,128)(2,1)}), bf16[32,16,2048]{2,1,0:T(8,128)(2,1)S(1)}, u32[]{:S(2)}, u32[]{:S(2)}) async-start(bf16[32,16,2048]{2,1,0:T(8,128)(2,1)} %bitcast.65), calls=%async_computation.1 | async-start | bytes 4194304 | tf_op jit(solution)/shard_map/all_to_all | solution.py:355
  199.2 2.9 %reduce_sum.44 = bf16[128,2048]{1,0:T(8,128)(2,1)} reduce(bf16[4,128,2048]{2,1,0:T(8,128)(2,1)} %copy-done.1, bf16[]{:T(256)} %constant.48.clone.1), dimensions={0}, to_apply=%region_5.6 | reduce | flops 786432 | bytes 2621442 | tf_op jit(solution)/shard_map/reduce_sum | solution.py:348
  202.1 25.5 %all-to-all-done.1 = bf16[32,16,2048]{2,1,0:T(8,128)(2,1)S(1)} async-done(((bf16[32,16,2048]{2,1,0:T(8,128)(2,1)}), bf16[32,16,2048]{2,1,0:T(8,128)(2,1)S(1)}, u32[]{:S(2)}, u32[]{:S(2)}) %all-to-all-start.1) | async-done | bytes 2097184 | tf_op jit(solution)/shard_map/all_to_all | solution.py:355
  227.6 2.3 gather_fusion.1
  230.0 2.4 reshape.128
  232.3 3.9 %multiply_reduce_fusion = bf16[128,2048]{1,0:T(8,128)(2,1)} fusion(f32[128,2,2048]{2,1,0:T(2,128)S(1)} %reshape.128, f32[128,2]{1,0:T(8,128)S(1)} %copy.64), kind=kLoop, calls=%fused_computation.7 | loop fusion | flops 786432 | bytes 2622464 | tf_op jit(solution)/shard_map/reduce_sum | solution.py:358
  (54 shorter events, 3.3 us)
Async XLA Ops:
  7.2 97.7 %copy-start = (bf16[256,2048]{1,0:T(8,128)(2,1)S(1)}, bf16[256,2048]{1,0:T(8,128)(2,1)}, u32[]{:S(2)}) copy-start(bf16[256,2048]{1,0:T(8,128)(2,1)} %param.16) | copy-start | bytes 3145732
  7.2 2.3 copy-start.7
  7.2 5.3 %copy-start.2 = (bf16[128,2048]{1,0:T(8,128)(2,1)S(1)}, bf16[128,2048]{1,0:T(8,128)(2,1)}, u32[]{:S(2)}) copy-start(bf16[128,2048]{1,0:T(8,128)(2,1)} %param.17) | copy-start | bytes 1572868
  7.2 104.8 %all-gather.7.cloned.1.call-start = ((), (), s32[]{:S(2)}) async-start(), calls=%async_computation.3 | async-start | bytes 5242880 | tf_op jit(solution)/shard_map/all_gather | solution.py:321
  7.9 7.0 %copy-start.3 = (bf16[512,256]{1,0:T(8,128)(2,1)S(1)}, bf16[512,256]{1,0:T(8,128)(2,1)}, u32[]{:S(2)}) copy-start(bf16[512,256]{1,0:T(8,128)(2,1)} %param.13) | copy-start | bytes 786436
  7.9 110.6 %all-gather.5.cloned.1.call-start = ((), (), s32[]{:S(2)}) async-start(), calls=%async_computation.2 | async-start | bytes 5242880 | tf_op jit(solution)/shard_map/all_gather | solution.py:320
  8.7 163.7 %all-gather.9.cloned.1.call-start = ((), (), s32[]{:S(2)}) async-start(), calls=%async_computation.4 | async-start | bytes 5242880 | tf_op jit(solution)/shard_map/all_gather | solution.py:322
  12.7 3.1 %copy-start.4 = (bf16[512,256]{1,0:T(8,128)(2,1)S(1)}, bf16[512,256]{1,0:T(8,128)(2,1)}, u32[]{:S(2)}) copy-start(bf16[512,256]{1,0:T(8,128)(2,1)} %param.14) | copy-start | bytes 786436
  15.1 1.2 copy-start.5
  15.3 1.8 copy-start.6
  107.9 70.7 %all-to-all-start = ((bf16[4,128,2048]{2,1,0:T(8,128)(2,1)}), bf16[4,128,2048]{2,1,0:T(8,128)(2,1)S(1)}, u32[]{:S(2)}, u32[]{:S(2)}) async-start(bf16[4,128,2048]{2,1,0:T(8,128)(2,1)} %bitcast.19), calls=%async_computation | async-start | bytes 4194304 | tf_op jit(solution)/shard_map/all_to_all | solution.py:347
  178.6 1.4 copy-start.1
  178.6 20.5 %copy-start.8 = (f32[128,2]{0,1:T(2,128)S(1)}, f32[128,2]{0,1:T(2,128)}, u32[]{:S(2)}) copy-start(f32[128,2]{0,1:T(2,128)} %param.20) | copy-start | bytes 3076
  180.0 47.7 %all-to-all-start.1 = ((bf16[32,16,2048]{2,1,0:T(8,128)(2,1)}), bf16[32,16,2048]{2,1,0:T(8,128)(2,1)S(1)}, u32[]{:S(2)}, u32[]{:S(2)}) async-start(bf16[32,16,2048]{2,1,0:T(8,128)(2,1)} %bitcast.65), calls=%async_computation.1 | async-start | bytes 4194304 | tf_op jit(solution)/shard_map/all_to_all | solution.py:355
Sparse Core Ops, SparseCore 0:
  9.7 51.1 all-gather.6
  62.6 48.5 all-gather.4
  112.8 59.5 all-gather.8
